TPU v7x, 512 devices: a 8x2x16 block of a 8x8x16 slice. The times are simulated.
512 devices in a mesh: grp: 2 (over y), sp: 16 (over z), tp: 16 (over x, core).
Axes of the slice: x: 8, y: 2, z: 16, core: 2. Of those that a mesh axis runs over, the one named last changes fastest.
The devices are a block of a 8x8x16 slice.
Arguments:
- latents: bfloat16 [12288, 4096], P(('grp', 'sp', 'tp')), parts along dimension 0, may hold values from -3 to 3
- conditions: float32 [4, 4096], P('grp', 'sp'), parts along dimension 0, may hold values from -6 to 6
- context: bfloat16 [1024, 4096], P(('grp', 'sp')), parts along dimension 0, may hold values from -6 to 6
- w_shift: bfloat16 [4096, 4096], P('sp', 'tp'), may hold values from -0.09375 to 0.09375
- w_scale: bfloat16 [4096, 4096], P('sp', 'tp'), may hold values from -0.09375 to 0.09375
- w_gate: bfloat16 [4096, 4096], P('sp', 'tp'), may hold values from -0.09375 to 0.09375
- w_qdown: bfloat16 [4096, 1024], P(None, 'tp'), may hold values from -2 to 2
- w_kvdown: bfloat16 [4096, 512], P(None, 'tp'), may hold values from -2 to 2
- w_rope: bfloat16 [4096, 32], replicated, may hold values from -0.09375 to 0.09375
- q_gain: float32 [1024], replicated, may hold values from 1 to 24
- latent_norm_gain: float32 [512], replicated, may hold values from 0.1 to 1.9
- query_up_weight: bfloat16 [1024, 3072], P(None, 'tp'), may hold values from -0.1875 to 0.1875
- key_up_weight: bfloat16 [512, 2048], P(None, 'tp'), may hold values from -0.25 to 0.25
- value_up_weight: bfloat16 [512, 2048], P(None, 'tp'), may hold values from -0.25 to 0.25
- context_bias: float32 [32], P('tp'), may hold values from 0.5 to 2
- w_out: bfloat16 [2048, 4096], P(None, 'tp'), may hold values from -0.5 to 0.5
Outputs:
- mixed: bfloat16 [12288, 4096], P(('grp', 'sp', 'tp')), parts along dimension 0
There are 2 independent parts, one for each index of `grp`. A program takes and returns all parts, laid end to end along the dimension named above; an argument that names none is the same for every part. Nothing has to cross between parts.
All inputs are finite; a program needn't handle non-finite values.
Results may differ from a plain program's by a relative error of at most 0.01345.
The roundings to bfloat16 on the way count: a program that leaves them out, or rounds other values in their place, can miss the bound.
Values may be sent and summed in bfloat16 or wider, within the bound.
A program may use at most 64 MiB of HBM per device.

v0:
```python
import jax
import jax.numpy as jnp
from jax import lax
from jax.sharding import PartitionSpec as P

PLAIN_QK_DIM = 64
ROTARY_DIM = 32
VALUE_DIM = 64
GRID_W = 64


EPSILON = 1e-06
NEGATIVE = -1e30


def sent_to_all(shard, axis):
    peers = lax.axis_size(axis)
    return lax.all_to_all(
        jnp.broadcast_to(shard[None], (peers, *shard.shape)), axis, 0, 0, tiled=True
    )


def over_copies(shard, axis):
    everything = sent_to_all(shard, axis)
    return jnp.sum(everything, axis=0)


def in_one_piece(arrays, axis, dim, along):
    ends, at = ([], 0)
    for a in arrays[:-1]:
        at += a.shape[along]
        ends.append(at)
    both = jnp.concatenate(arrays, axis=along)
    return tuple(jnp.split(lax.all_gather(both, axis, axis=dim, tiled=True), ends, axis=along))


def layer_modulate(row_block, shift_by, scale_by):
    values = row_block.astype(jnp.float32)
    center = values - jnp.mean(values, axis=-1, keepdims=True)
    spread = jnp.mean(center * center, axis=-1, keepdims=True)
    normed = center * lax.rsqrt(spread + EPSILON)
    return (normed * (1.0 + scale_by) + shift_by).astype(jnp.bfloat16)


def rms_scale(raw_rows, gain_vec):
    values = raw_rows.astype(jnp.float32)
    factor = lax.rsqrt(jnp.mean(values * values, axis=-1, keepdims=True) + EPSILON)
    return (values * factor * gain_vec).astype(jnp.bfloat16)


def axial_turn(values, positions):
    freq_count = values.shape[-1] // 4
    inverse = 10000.0 ** (-jnp.arange(freq_count, dtype=jnp.float32) / freq_count)
    grid_row = (positions // GRID_W).astype(jnp.float32)
    grid_col = (positions % GRID_W).astype(jnp.float32)
    target = (positions.shape[0],) + (1,) * (values.ndim - 2) + (freq_count,)
    pieces = []
    for half_index, coordinate in enumerate((grid_row, grid_col)):
        angles = (coordinate[:, None] * inverse[None, :]).reshape(target)
        cosine = jnp.cos(angles)
        sine_of = jnp.sin(angles)
        segment = values[..., 2 * half_index * freq_count : 2 * (half_index + 1) * freq_count]
        low_half = segment[..., :freq_count]
        high_half = segment[..., freq_count:]
        pieces.append(low_half * cosine - high_half * sine_of)
        pieces.append(low_half * sine_of + high_half * cosine)
    return jnp.concatenate(pieces, axis=-1)


def on_device(
    latents,
    conditions,
    context,
    w_shift,
    w_scale,
    w_gate,
    w_qdown,
    w_kvdown,
    w_rope,
    q_gain,
    latent_norm_gain,
    query_up_weight,
    key_up_weight,
    value_up_weight,
    context_bias,
    w_out,
):
    tp_count = lax.axis_size("tp")
    tp_index = lax.axis_index("tp")
    sp_index = lax.axis_index("sp")
    own_rows = latents.shape[0]
    tok_count = own_rows * tp_count
    ctx_share = context.shape[0] // tp_count
    cond_act = jax.nn.silu(conditions).astype(jnp.bfloat16)
    partial_mod = jnp.concatenate(
        [
            jnp.dot(cond_act, w_shift, preferred_element_type=jnp.float32),
            jnp.dot(cond_act, w_scale, preferred_element_type=jnp.float32),
            jnp.dot(cond_act[0:1], w_gate, preferred_element_type=jnp.float32),
        ],
        axis=0,
    )
    summed = over_copies(partial_mod, "sp")
    modulation = lax.all_gather(summed, "tp", axis=1, tiled=True)
    ctx_own = lax.dynamic_slice_in_dim(context, tp_index * ctx_share, ctx_share, 0)
    h_lat = layer_modulate(latents, modulation[0], modulation[2])
    h_ctx = layer_modulate(ctx_own, modulation[1], modulation[3])
    h_own = jnp.concatenate([h_lat, h_ctx], axis=0)
    rope_raw = jnp.dot(h_own, w_rope, preferred_element_type=jnp.float32)
    own_pos = sp_index * tok_count + tp_index * own_rows + jnp.arange(own_rows, dtype=jnp.int32)
    kr_lat = axial_turn(rope_raw[:own_rows], own_pos).astype(jnp.bfloat16)
    kr_ctx = rope_raw[own_rows:].astype(jnp.bfloat16)
    arrived = lax.all_gather(h_own, "tp", axis=0, tiled=True)
    projected = jnp.concatenate(
        [
            jnp.dot(arrived, w_qdown, preferred_element_type=jnp.float32),
            jnp.dot(arrived, w_kvdown, preferred_element_type=jnp.float32),
        ],
        axis=1,
    ).astype(jnp.bfloat16)
    q_cols = w_qdown.shape[1]
    grouped = projected.reshape(tp_count, own_rows + ctx_share, projected.shape[1])
    cq_cols = grouped[:, :own_rows, :q_cols].reshape(tok_count, q_cols)
    kvl_cols = grouped[:, :own_rows, q_cols:].reshape(tok_count, w_kvdown.shape[1])
    kvc_cols = grouped[:, own_rows:, q_cols:].reshape(tp_count * ctx_share, w_kvdown.shape[1])
    cq_raw, kvl_raw, kvc_raw, krl_all, krc_all = (
        lax.all_gather(cq_cols, "tp", axis=1, tiled=True),
        *in_one_piece((kvl_cols, kvc_cols), "tp", 1, 0),
        lax.all_gather(kr_lat, "tp", axis=0, tiled=True),
        lax.all_gather(kr_ctx, "tp", axis=0, tiled=True),
    )
    cq_all = rms_scale(cq_raw, q_gain)
    ckv_all = jnp.concatenate(
        [rms_scale(kvl_raw, latent_norm_gain), rms_scale(kvc_raw, latent_norm_gain)], axis=0
    )
    kr_all = jnp.concatenate([krl_all, krc_all], axis=0)
    head_count = query_up_weight.shape[1] // (PLAIN_QK_DIM + ROTARY_DIM)
    q_all = jnp.dot(cq_all, query_up_weight, preferred_element_type=jnp.float32)
    q_all = q_all.reshape(tok_count, head_count, PLAIN_QK_DIM + ROTARY_DIM)
    query_pos = sp_index * tok_count + jnp.arange(tok_count, dtype=jnp.int32)
    queries = jnp.concatenate(
        [q_all[..., :PLAIN_QK_DIM], axial_turn(q_all[..., PLAIN_QK_DIM:], query_pos)], axis=-1
    ).astype(jnp.bfloat16)
    q_nope = queries[..., :PLAIN_QK_DIM]
    q_rope = queries[..., PLAIN_QK_DIM:]
    seg_rows = ckv_all.shape[0]
    is_ctx = (jnp.arange(seg_rows, dtype=jnp.int32) >= tok_count).astype(jnp.float32)
    bias_row = context_bias[None, :, None] * is_ctx[None, None, :]
    score_scale = (PLAIN_QK_DIM + ROTARY_DIM) ** (-0.5)

    def attend_block(running, key_block, value_block, rope_block):
        running_max, running_sum, numerator = running
        scores = jnp.einsum("ihd,jhd->ihj", q_nope, key_block, preferred_element_type=jnp.float32)
        scores = scores + jnp.einsum(
            "ihd,jd->ihj", q_rope, rope_block, preferred_element_type=jnp.float32
        )
        scores = scores * score_scale + bias_row
        new_max = jnp.maximum(running_max, jnp.max(scores, axis=-1))
        rescale = jnp.exp(running_max - new_max)
        exponent = jnp.exp(scores - new_max[..., None])
        running_sum = running_sum * rescale + jnp.sum(exponent, axis=-1)
        numerator = numerator * rescale[..., None] + jnp.einsum(
            "ihj,jhd->ihd",
            exponent.astype(jnp.bfloat16),
            value_block,
            preferred_element_type=jnp.float32,
        )
        return (new_max, running_sum, numerator)

    initial = (
        jnp.full((tok_count, head_count), NEGATIVE, jnp.float32),
        jnp.zeros((tok_count, head_count), jnp.float32),
        jnp.zeros((tok_count, head_count, VALUE_DIM), jnp.float32),
    )
    keys_own = jnp.dot(ckv_all, key_up_weight, preferred_element_type=jnp.float32).astype(
        jnp.bfloat16
    )
    values_own = jnp.dot(ckv_all, value_up_weight, preferred_element_type=jnp.float32).astype(
        jnp.bfloat16
    )

    def expand_heads(key_group):
        key_flat, value_flat, rope_block = key_group
        return (
            key_flat.reshape(seg_rows, head_count, PLAIN_QK_DIM),
            value_flat.reshape(seg_rows, head_count, VALUE_DIM),
            rope_block,
        )

    members = in_one_piece((keys_own, values_own, kr_all), "sp", 0, 1)
    block_count = members[0].shape[0] // seg_rows
    stacked = tuple(
        (member.reshape((block_count, seg_rows) + member.shape[1:]) for member in members)
    )

    def step_fn(state, key_group):
        key_block, value_block, rope_block = expand_heads(key_group)
        return (attend_block(state, key_block, value_block, rope_block), None)

    result, unused = lax.scan(step_fn, initial, stacked)
    running_max, running_sum, numerator = result
    attended = (
        (numerator / running_sum[..., None])
        .astype(jnp.bfloat16)
        .reshape(tok_count, head_count * VALUE_DIM)
    )
    proj_cols = jnp.dot(
        lax.all_gather(attended, "tp", axis=1, tiled=True),
        w_out,
        preferred_element_type=jnp.float32,
    )
    proj_rows = lax.all_to_all(
        proj_cols.astype(jnp.bfloat16), "tp", split_axis=0, concat_axis=1, tiled=True
    )
    mixed_rows = latents.astype(jnp.float32) + modulation[4] * proj_rows.astype(jnp.float32)
    return mixed_rows.astype(jnp.bfloat16)


def solution(mesh):
    in_specs = (
        P(("grp", "sp", "tp"), None),
        P("grp", "sp"),
        P(("grp", "sp"), None),
        P("sp", "tp"),
        P("sp", "tp"),
        P("sp", "tp"),
        P(None, "tp"),
        P(None, "tp"),
        P(),
        P(),
        P(),
        P(None, "tp"),
        P(None, "tp"),
        P(None, "tp"),
        P("tp"),
        P(None, "tp"),
    )
    out_specs = P(("grp", "sp", "tp"), None)
    return jax.shard_map(
        on_device, mesh=mesh, in_specs=in_specs, out_specs=out_specs, check_vma=False
    )
```

profile of v0, /device:TPU:65, one launch (start us, length us, event | category | flops | bytes accessed | tf_op | source)
XLA Modules:
  0.0 374.4 jit_solution(4335878256825156136)
XLA Ops:
  7.4 1.0 fusion.77
  8.4 1.1 fusion.78
  9.5 1.1 fusion.66
  11.2 44.2 %all-to-all-start = ((f32[16,5,256]{2,1,0:T(8,128)}), f32[16,5,256]{2,1,0:T(8,128)S(1)}, u32[]{:S(2)}, u32[]{:S(2)}) async-start(f32[16,5,256]{2,1,0:T(8,128)} %broadcast_in_dim.8), calls=%async_computation | async-start | bytes 262144 | tf_op jit(solution)/shard_map/all_to_all | solution.py:18
  55.5 1.0 convert_reduce_fusion.1
  56.5 1.1 fusion.39
  57.6 1.1 convert_reduce_fusion
  58.7 1.2 fusion.27
  59.8 7.4 %all-to-all-done = f32[16,5,256]{2,1,0:T(8,128)S(1)} async-done(((f32[16,5,256]{2,1,0:T(8,128)}), f32[16,5,256]{2,1,0:T(8,128)S(1)}, u32[]{:S(2)}, u32[]{:S(2)}) %all-to-all-start) | async-done | bytes 81952 | tf_op jit(solution)/shard_map/all_to_all | solution.py:18
  67.2 21.9 %all_gather.24 = f32[5,4096]{1,0:T(8,128)S(1)} all-gather(f32[5,256]{1,0:T(8,128)S(1)} %reduce_sum.81), channel_id=1, replica_groups=mesh['grp'=2,'sp'=16,'tp'=16] {'tp'}, dimensions={1}, use_global_device_ids=true | all-gather | bytes 87040 | tf_op jit(solution)/shard_map/all_gather | solution.py:104
  92.0 14.9 %all-gather.1 = bf16[16,2,32]{2,1,0:T(2,128)(2,1)S(1)} all-gather(bf16[1,2,32]{2,1,0:T(2,128)(2,1)S(1)} %fusion.67), channel_id=1, replica_groups=mesh['grp'=2,'sp'=16,'tp'=16] {'tp'}, dimensions={0}, use_global_device_ids=true | all-gather | bytes 2176 | tf_op jit(solution)/shard_map/all_gather | solution.py:130
  106.9 15.8 %all_gather.27 = bf16[384,32]{1,0:T(8,128)(2,1)S(1)} all-gather(bf16[24,32]{1,0:T(8,128)(2,1)S(1)} %copy.106), channel_id=1, replica_groups=mesh['grp'=2,'sp'=16,'tp'=16] {'tp'}, dimensions={0}, use_global_device_ids=true | all-gather | bytes 26112 | tf_op jit(solution)/shard_map/all_gather | solution.py:129
  122.7 7.8 %all-gather.9.cloned.1.call-done = bf16[16,26,4096]{2,1,0:T(8,128)(2,1)} async-done(((bf16[1,26,4096]{2,1,0:T(8,128)(2,1)}), bf16[16,26,4096]{2,1,0:T(8,128)(2,1)}) %all-gather.9.cloned.1.call-update) | async-done | bytes 3407888 | tf_op jit(solution)/shard_map/all_gather | solution.py:113
  130.5 4.9 %reshape.337 = bf16[416,4096]{1,0:T(8,128)(2,1)} reshape(bf16[16,26,4096]{2,1,0:T(8,128)(2,1)} %all-gather.9.cloned.1.call-done) | data formatting | bytes 6815744
  135.5 3.0 convolution_convert_fusion.4
  139.3 18.1 %all_gather.26 = bf16[416,512]{0,1:T(8,128)(2,1)S(1)} all-gather(bf16[416,32]{0,1:T(8,128)(2,1)S(1)} %pad_maximum_fusion.6), channel_id=1, replica_groups=mesh['grp'=2,'sp'=16,'tp'=16] {'tp'}, dimensions={1}, use_global_device_ids=true | all-gather | bytes 452608 | tf_op jit(solution)/shard_map/all_gather | solution.py:34
  159.9 3.1 convolution_convert_fusion.3
  163.3 16.7 %all_gather.30 = bf16[384,1024]{0,1:T(8,128)(2,1)S(1)} all-gather(bf16[384,64]{0,1:T(8,128)(2,1)S(1)} %copy.110), channel_id=1, replica_groups=mesh['grp'=2,'sp'=16,'tp'=16] {'tp'}, dimensions={1}, use_global_device_ids=true | all-gather | bytes 835584 | tf_op jit(solution)/shard_map/all_gather | solution.py:127
  180.8 49.6 %all-gather.11.cloned.1.call-done = bf16[16,416,288]{1,2,0:T(8,128)(2,1)} async-done(((bf16[1,416,288]{1,2,0:T(8,128)(2,1)}), bf16[16,416,288]{1,2,0:T(8,128)(2,1)}) %all-gather.11.cloned.1.call-update) | async-done | bytes 3833872 | tf_op jit(solution)/shard_map/all_gather | solution.py:34
  230.4 7.8 %copy.108 = bf16[16,416,288]{2,1,0:T(8,128)(2,1)} copy(bf16[16,416,288]{1,2,0:T(8,128)(2,1)} %all-gather.11.cloned.1.call-done) | data formatting | bytes 7667712 | tf_op jit(solution)/shard_map/all_gather | solution.py:34
  238.2 3.9 %fusion.74 = (bf16[6656,128]{1,0:T(8,128)(2,1)}, bf16[6656,128]{1,0:T(8,128)(2,1)}) fusion(bf16[6656,288]{1,0:T(8,128)(2,1)} %bitcast.95), kind=kLoop, calls=%fused_computation.147 | loop fusion | bytes 6815744 | tf_op jit(solution)/shard_map/split | solution.py:34
  242.1 1.6 split.23
  243.7 1.5 copy.113
  245.2 54.8 %while.15 = (s32[]{:T(128)}, f32[384,2]{0,1:T(2,128)S(1)}, f32[384,2]{0,1:T(2,128)S(1)}, f32[384,2,64]{0,2,1:T(8,128)S(1)}, bf16[16,416,128]{2,1,0:T(8,128)(2,1)...) while((s32[]{:T(128)}, f32[384,2]{0,1:T(2,128)S(1)}, ...), condition=%wide.region_11.12_spmd.clone, body=%wide.region_8.11_spmd.clone.sunk | while | flops 104944192 | bytes 8086293 | solution.py:200
  246.2 1.1 convolution_bitcast_fusion.4
  248.6 1.0 constant_dynamic-slice_fusion.3
  249.7 1.1 convolution_bitcast_fusion.4
  252.0 1.0 constant_dynamic-slice_fusion.3
  253.1 1.1 convolution_bitcast_fusion.4
  255.4 1.0 constant_dynamic-slice_fusion.3
  256.5 1.1 convolution_bitcast_fusion.4
  258.9 1.0 constant_dynamic-slice_fusion.3
  259.9 1.1 convolution_bitcast_fusion.4
  262.3 1.0 constant_dynamic-slice_fusion.3
  263.4 1.1 convolution_bitcast_fusion.4
  266.8 1.1 convolution_bitcast_fusion.4
  270.2 1.1 convolution_bitcast_fusion.4
  273.7 1.1 convolution_bitcast_fusion.4
  277.1 1.1 convolution_bitcast_fusion.4
  280.5 1.1 convolution_bitcast_fusion.4
  283.9 1.1 convolution_bitcast_fusion.4
  287.4 1.1 convolution_bitcast_fusion.4
  290.8 1.1 convolution_bitcast_fusion.4
  294.2 1.1 convolution_bitcast_fusion.4
  297.6 1.1 convolution_bitcast_fusion.4
  300.7 49.4 %all-gather.7.cloned.1.call-done = bf16[384,2048]{0,1:T(8,128)(2,1)} async-done(((bf16[384,128]{0,1:T(8,128)(2,1)}), bf16[384,2048]{0,1:T(8,128)(2,1)}) %all-gather.7.cloned.1.call-update) | async-done | bytes 1572880 | tf_op jit(solution)/shard_map/all_gather | solution.py:208
  350.1 2.0 convolution_convert_fusion
  352.1 14.9 %all_to_all.18 = bf16[16,24,256]{2,1,0:T(8,128)(2,1)S(1)} all-to-all(bf16[16,24,256]{2,1,0:T(8,128)(2,1)S(1)} %bitcast.104), channel_id=1, replica_groups=mesh['grp'=2,'sp'=16,'tp'=16] {'tp'}, dimensions={0} | all-to-all | bytes 393216 | tf_op jit(solution)/shard_map/all_to_all | solution.py:212
  (243 shorter events, 41.1 us)
Async XLA Ops:
  6.5 343.5 %copy-start = (bf16[2048,256]{1,0:T(8,128)(2,1)S(1)}, bf16[2048,256]{1,0:T(8,128)(2,1)}, u32[]{:S(2)}) copy-start(bf16[2048,256]{1,0:T(8,128)(2,1)} %param.33) | copy-start | bytes 3145732
  6.6 83.6 %copy-start.1 = (bf16[24,4096]{1,0:T(8,128)(2,1)S(1)}, bf16[24,4096]{1,0:T(8,128)(2,1)}, u32[]{:S(2)}) copy-start(bf16[24,4096]{1,0:T(8,128)(2,1)} %param.18) | copy-start | bytes 589828
  6.6 84.7 %copy-start.7 = (bf16[4096,32]{0,1:T(8,128)(2,1)S(1)}, bf16[4096,32]{0,1:T(8,128)(2,1)}, u32[]{:S(2)}) copy-start(bf16[4096,32]{0,1:T(8,128)(2,1)} %param.26) | copy-start | bytes 786436
  11.2 56.0 %all-to-all-start = ((f32[16,5,256]{2,1,0:T(8,128)}), f32[16,5,256]{2,1,0:T(8,128)S(1)}, u32[]{:S(2)}, u32[]{:S(2)}) async-start(f32[16,5,256]{2,1,0:T(8,128)} %broadcast_in_dim.8), calls=%async_computation | async-start | bytes 262144 | tf_op jit(solution)/shard_map/all_to_all | solution.py:18
  55.4 75.1 %all-gather.9.cloned.1.call-start = ((), (), s32[]{:S(2)}) async-start(), calls=%async_computation.3 | async-start | bytes 4456448 | tf_op jit(solution)/shard_map/all_gather | solution.py:113
  91.1 139.3 %all-gather.11.cloned.1.call-start = ((), (), s32[]{:S(2)}) async-start(), calls=%async_computation.4 | async-start | bytes 5013504 | tf_op jit(solution)/shard_map/all_gather | solution.py:34
  122.7 12.7 %copy-start.3 = (bf16[4096,32]{0,1:T(8,128)(2,1)S(1)}, bf16[4096,32]{0,1:T(8,128)(2,1)}, u32[]{:S(2)}) copy-start(bf16[4096,32]{0,1:T(8,128)(2,1)} %param.25) | copy-start | bytes 786436
  138.5 19.1 %copy-start.5 = (f32[512]{0:T(512)S(1)}, f32[512]{0:T(512)}, u32[]{:S(2)}) copy-start(f32[512]{0:T(512)} %param.28) | copy-start | bytes 6148
  138.5 19.4 %copy-start.8 = (bf16[512,128]{1,0:T(8,128)(2,1)S(1)}, bf16[512,128]{1,0:T(8,128)(2,1)}, u32[]{:S(2)}) copy-start(bf16[512,128]{1,0:T(8,128)(2,1)} %param.30) | copy-start | bytes 393220
  139.3 18.9 %copy-start.9 = (bf16[512,128]{1,0:T(8,128)(2,1)S(1)}, bf16[512,128]{1,0:T(8,128)(2,1)}, u32[]{:S(2)}) copy-start(bf16[512,128]{1,0:T(8,128)(2,1)} %param.31) | copy-start | bytes 393220
  158.2 1.6 copy-start.2
  159.6 190.5 %all-gather.7.cloned.1.call-start = ((), (), s32[]{:S(2)}) async-start(), calls=%async_computation.2 | async-start | bytes 1671168 | tf_op jit(solution)/shard_map/all_gather | solution.py:208
  162.9 17.3 %copy-start.6 = (bf16[1024,192]{0,1:T(8,128)(2,1)S(1)}, bf16[1024,192]{0,1:T(8,128)(2,1)}, u32[]{:S(2)}) copy-start(bf16[1024,192]{0,1:T(8,128)(2,1)} %param.29) | copy-start | bytes 1179652
  163.0 17.3 %copy-start.10 = (f32[1024]{0:T(1024)S(1)}, f32[1024]{0:T(1024)}, u32[]{:S(2)}) copy-start(f32[1024]{0:T(1024)} %param.27) | copy-start | bytes 12292
  243.7 1.5 copy-start.4
Sparse Core Ops, SparseCore 0:
  91.2 39.2 all-gather.8
  159.7 70.6 all-gather.10
  300.8 49.2 all-gather.6
where the time goes:
time: 377 us; the launch traced here: 374 us
  waiting for transfers between devices  114 us (30%)
  blocking collectives  102 us (27%)
  starting transfers between devices  44.4 us (12%)
  matrix products  42.6 us (11%)
  local copies, waits for them, and re-layouts  41.9 us (11%)
  other arithmetic  14.3 us (4%)
  between operations  13.5 us (4%)
    all_gather x1, waiting for transfers between devices, in_one_piece(): lax.all_gather(both, axis, axis=dim, tiled=True)  49.6 us
    all_gather x1, waiting for transfers between devices, on_device(): lax.all_gather(attended, 'tp', axis=1, tiled=True)  49.4 us
    all_to_all x1, starting transfers between devices, sent_to_all(): lax.all_to_all(jnp.broadcast_to(shard[None], (peers, *shard.shape)), axis...  44.2 us
    all_gather x1, blocking collectives, on_device(): modulation = lax.all_gather(summed, 'tp', axis=1, tiled=True)  21.9 us
    dynamic_slice x48, local copies, waits for them, and re-layouts, on_device(): result, unused = lax.scan(step_fn, initial, stacked)  19.1 us
    all_gather x1, blocking collectives, in_one_piece(): lax.all_gather(both, axis, axis=dim, tiled=True)  18.1 us
    dot_general x16, matrix products, attend_block(): jnp.einsum('ihd,jd->ihj', q_rope, rope_block, preferred_element_type=jnp....  17.9 us
    all_gather x1, blocking collectives, on_device(): lax.all_gather(cq_cols, 'tp', axis=1, tiled=True)  16.7 us
  transfers between devices with their start and end apart: 4, of which 4 were waited for; matrix products, arithmetic and copies ran while one was open for 3% of the time, Pallas kernels for 0%

commit v1 on v0

v1 whole, which is shorter than its diff:
```python
import functools
import math

import jax
import jax.numpy as jnp
from jax import lax
from jax.experimental import pallas as pl
from jax.experimental.pallas import tpu as pltpu
from jax.sharding import PartitionSpec as P

PLAIN = 64
ROTARY = 32
VALUE = 64
GRID_W = 64
EPSILON = 1e-6
NEGATIVE = -1e30
LOG2E = 1.4426950408889634
SCORE = (PLAIN + ROTARY) ** (-0.5)
MESH = pl.DeviceIdType.MESH
BF = jnp.bfloat16
F32 = jnp.float32
KROWS = 2 * PLAIN + ROTARY
VROWS = 2 * VALUE


class Gather:
    def __init__(self, count, place, towards, chunks, sems, partner=None, core=0):
        self.count, self.place, self.towards = count, place, towards
        self.chunks, self.partner, self.core = chunks, partner, core
        self.recv, self.send = sems[0], sems[1]
        self.pair_recv, self.pair_send = (sems[2], sems[3]) if partner is not None else (None, None)
        self.reach = count // 2
        self.cut = (len(chunks) + 1) // 2

    def active(self, d, s, ch):
        if s < self.reach:
            return True
        if s > self.reach:
            return False
        return (ch < self.cut) if d == 0 else (ch >= self.cut)

    def source(self, d, s):
        move = (self.count - s) if d == 0 else s
        return lax.rem(self.place + move, self.count)

    def ring_copy(self, d, s, ch):
        piece = self.chunks[ch](self.source(d, s), self.core)
        return pltpu.make_async_remote_copy(
            src_ref=piece, dst_ref=piece, send_sem=self.send.at[d, s, ch], recv_sem=self.recv.at[d, s + 1, ch],
            device_id=self.towards(1 if d == 0 else self.count - 1), device_id_type=MESH)

    def ring_arrival(self, d, s, ch):
        piece = self.chunks[ch](self.source(d, s), self.core)
        return pltpu.make_async_remote_copy(
            src_ref=piece, dst_ref=piece, send_sem=self.send.at[d, s, ch], recv_sem=self.recv.at[d, s, ch],
            device_id=self.towards(self.count - 1 if d == 0 else 1), device_id_type=MESH)

    def pair_copy(self, d, s, ch, core):
        piece = self.chunks[ch](self.source(d, s), core)
        return pltpu.make_async_remote_copy(
            src_ref=piece, dst_ref=piece, send_sem=self.pair_send.at[d, s, ch], recv_sem=self.pair_recv.at[d, s, ch],
            device_id=self.partner, device_id_type=MESH)

    def start(self, only=None):
        for ch in range(len(self.chunks)) if only is None else only:
            for d in range(2):
                if self.active(d, 1, ch):
                    self.ring_copy(d, 0, ch).start()
            if self.partner is not None:
                self.pair_copy(0, 0, ch, self.core).start()

    def step(self, s):
        for ch in range(len(self.chunks)):
            for d in range(2):
                if self.active(d, s, ch):
                    self.ring_arrival(d, s, ch).wait_recv()
                    if self.active(d, s + 1, ch):
                        self.ring_copy(d, s, ch).start()
                    if self.partner is not None:
                        self.pair_copy(d, s, ch, self.core).start()

    def pair_step(self, s, only=None):
        for ch in range(len(self.chunks)) if only is None else only:
            for d in range(2):
                if (s == 0 and d == 0) or (s > 0 and self.active(d, s, ch)):
                    self.pair_copy(d, s, ch, 1 - self.core).wait_recv()

    def finish(self):
        for s in range(self.reach + 1):
            for ch in range(len(self.chunks)):
                for d in range(2):
                    if self.active(d, s + 1, ch):
                        self.ring_copy(d, s, ch).wait_send()
                    if self.partner is not None and ((s == 0 and d == 0) or (s > 0 and self.active(d, s, ch))):
                        self.pair_copy(d, s, ch, self.core).wait_send()


def axial_turn(a, row_cos, row_sin, col_cos, col_sin):
    a0, a1, a2, a3 = a[0:8], a[8:16], a[16:24], a[24:32]
    return jnp.concatenate(
        [a0 * row_cos - a1 * row_sin, a0 * row_sin + a1 * row_cos,
         a2 * col_cos - a3 * col_sin, a2 * col_sin + a3 * col_cos], axis=0)


def modulated(block, shift, scale):
    values = block.astype(F32)
    center = values - jnp.mean(values, axis=-1, keepdims=True)
    spread = jnp.mean(center * center, axis=-1, keepdims=True)
    return (center * lax.rsqrt(spread + EPSILON) * (1.0 + scale) + shift).astype(BF)


def rms_columns(raw, gain):
    values = raw.astype(F32)
    factor = lax.rsqrt(jnp.mean(values * values, axis=0, keepdims=True) + EPSILON)
    return (values * factor * gain).astype(BF)


def kernel(nz, nt, *refs):
    (lat_hbm, cond_ref, ctx_hbm, wsh_ref, wsc_ref, wg_ref, wq_hbm, wkv_hbm, wr_hbm, qg_ref, kg_ref,
     uq_hbm, uk_hbm, uv_hbm, bias_ref, wo_hbm, out_ref,
     lat, ctx, own_lat, wq, wkv, wr, uq, uk, uv, wo,
     wcat, uqT, ukvT, zmod, xmod, mod, h, hc, qraw, kvraw, kvcraw, kv, kvc, qb,
     m_ref, l_ref, acc, att, pbuf, mbuf,
     load_sem, zm_s, zm_r, xm_s, xm_r, a_s, a_r, lat_x, ctx_z, raw_x, rawc_x, kv_z, att_x) = refs
    z, t = lax.axis_index("sp"), lax.axis_index("tp")
    core = lax.rem(t, 2)
    chip = t // 2
    nx = nt // 2
    rows = own_lat.shape[0]
    tok = rows * nt
    crows = ctx.shape[1]
    width = own_lat.shape[1]
    part = width // nt
    rank_q, rank_kv = wq.shape[1], wkv.shape[1]
    along_z = lambda k: {"sp": lax.rem(z + k, nz)}
    along_x = lambda k: {"tp": lax.rem(t + 2 * k, nt)}
    partner = {"tp": t + 1 - 2 * core}
    half = width // 2

    loads = [
        pltpu.make_async_copy(lat_hbm, lat.at[t], load_sem.at[0]),
        pltpu.make_async_copy(ctx_hbm, ctx.at[z], load_sem.at[1]),
        pltpu.make_async_copy(lat_hbm, own_lat, load_sem.at[2]),
        pltpu.make_async_copy(wq_hbm, wq, load_sem.at[3]),
        pltpu.make_async_copy(wkv_hbm, wkv, load_sem.at[4]),
        pltpu.make_async_copy(wr_hbm, wr, load_sem.at[5]),
        pltpu.make_async_copy(uq_hbm, uq, load_sem.at[6]),
        pltpu.make_async_copy(uk_hbm, uk, load_sem.at[7]),
        pltpu.make_async_copy(uv_hbm, uv, load_sem.at[8]),
        pltpu.make_async_copy(wo_hbm, wo, load_sem.at[9]),
    ]
    barrier = pltpu.get_barrier_semaphore()
    for k in range(1, nz):
        pl.semaphore_signal(barrier, inc=1, device_id=along_z(k), device_id_type=MESH)
    for k in range(1, nt):
        pl.semaphore_signal(barrier, inc=1, device_id={"tp": lax.rem(t + k, nt)}, device_id_type=MESH)
    for load in loads:
        load.start()

    cond = cond_ref[...]
    act = cond / (1.0 + jnp.exp(-cond))
    act = jnp.concatenate([act, jnp.zeros((14, act.shape[1]), F32)], axis=0).astype(BF)
    shift_part = jnp.dot(act, wsh_ref[...], preferred_element_type=F32)
    scale_part = jnp.dot(act, wsc_ref[...], preferred_element_type=F32)
    gate_part = jnp.dot(act, wg_ref[...], preferred_element_type=F32)
    zmod[z] = jnp.concatenate([shift_part[0:2], scale_part[0:2], gate_part[0:2], gate_part[2:4]], axis=0)
    pl.semaphore_wait(barrier, nz + nt - 2)

    def zm(k, incoming):
        if incoming:
            src = lax.rem(z + nz - k, nz)
            return pltpu.make_async_remote_copy(zmod.at[src], zmod.at[src], zm_s.at[k], zm_r.at[k], device_id=along_z(nz - k), device_id_type=MESH)
        return pltpu.make_async_remote_copy(zmod.at[z], zmod.at[z], zm_s.at[k], zm_r.at[k], device_id=along_z(k), device_id_type=MESH)

    def xm(k, incoming):
        if incoming:
            src = lax.rem(t + nt - k, nt)
            return pltpu.make_async_remote_copy(xmod.at[src], xmod.at[src], xm_s.at[k], xm_r.at[k], device_id={"tp": src}, device_id_type=MESH)
        return pltpu.make_async_remote_copy(xmod.at[t], xmod.at[t], xm_s.at[k], xm_r.at[k], device_id={"tp": lax.rem(t + k, nt)}, device_id_type=MESH)

    order = sorted(range(1, nz), key=lambda k: -min(k, nz - k))
    for k in order:
        zm(k, False).start()
    loads[0].wait()
    lat_ring = Gather(nx, chip, along_x,
                      [lambda p, c: lat.at[2 * p + c, :, pl.ds(0, half)], lambda p, c: lat.at[2 * p + c, :, pl.ds(half, half)]],
                      lat_x, partner, core)
    lat_ring.start()
    loads[1].wait()
    quarter = half // 2
    at_half = lambda c, q: pl.ds(pl.multiple_of(c * half + q * quarter, 128), quarter)
    ctx_ring = Gather(nz, z, along_z,
                      [lambda p, c: ctx.at[p, :, at_half(c, 0)], lambda p, c: ctx.at[p, :, at_half(c, 1)]],
                      ctx_z, partner, core)
    for ch in range(2):
        for d in range(2):
            ctx_ring.ring_copy(d, 0, ch).start()

    for load in loads[2:]:
        load.wait()
    steps = 8
    depth = width // steps
    for i in range(steps):
        cut = pl.ds(i * depth, depth)
        wcat[cut, :] = jnp.concatenate([wq[cut, :], wkv[cut, :], wr[cut, :]], axis=1)
    uqT[...] = uq[...].astype(F32).T.astype(BF)
    ukvT[0:2 * PLAIN, :] = uk[...].astype(F32).T.astype(BF)
    ukvT[2 * PLAIN:2 * PLAIN + VROWS, :] = uv[...].astype(F32).T.astype(BF)
    q_gain = jnp.broadcast_to(qg_ref[...], (8, qg_ref.shape[1])).T[:, 0:1]
    kv_gain = jnp.broadcast_to(kg_ref[...], (8, kg_ref.shape[1])).T[:, 0:1]
    pos = lax.broadcasted_iota(jnp.int32, (8, tok), 1) + z * tok
    freq = jnp.exp(lax.broadcasted_iota(jnp.int32, (8, tok), 0).astype(F32) * (-math.log(10000.0) / 8))
    row_angle = (pos >> 6).astype(F32) * freq
    col_angle = (pos & (GRID_W - 1)).astype(F32) * freq
    turn = (jnp.cos(row_angle), jnp.sin(row_angle), jnp.cos(col_angle), jnp.sin(col_angle))

    for k in reversed(order):
        zm(k, True).wait_recv()
    total = zmod[0]
    for k in range(1, nz):
        total = total + zmod[k]
    xmod[t] = total
    for k in range(1, nt):
        xm(k, False).start()

    def ctx_step(s):
        for ch in range(2):
            for d in range(2):
                if ctx_ring.active(d, s, ch):
                    ctx_ring.ring_arrival(d, s, ch).wait_recv()
                    if ctx_ring.active(d, s + 1, ch):
                        ctx_ring.ring_copy(d, s, ch).start()
                    ctx_ring.pair_copy(d, s, ch, core).start()

    steps_z = list(range(1, ctx_ring.reach + 1))
    for s in range(1, lat_ring.reach + 1):
        lat_ring.step(s)
        for _ in range(1):
            if steps_z:
                ctx_step(steps_z.pop(0))
    for s in range(0, lat_ring.reach + 1):
        lat_ring.pair_step(s)
    for k in range(1, nt):
        xm(k, True).wait_recv()
    for j in range(nt):
        mod[:, j * part:(j + 1) * part] = xmod[j]

    @pl.loop(0, nt // 2)
    def _(i):
        block = jnp.concatenate([lat[2 * i].astype(F32), lat[2 * i + 1].astype(F32)], axis=0)
        at = pl.ds(pl.multiple_of(i * 2 * rows, 2 * rows), 2 * rows)
        h[at, :] = modulated(block, mod[0:1, :], mod[2:3, :])

    raw = jnp.dot(h[...], wcat[...], preferred_element_type=F32).T
    q_at = lambda p, c, i: pl.ds(pl.multiple_of((2 * p + c) * rank_q + i * (rank_q // 2), rank_q // 2), rank_q // 2)
    kv_at = lambda p, c: pl.ds(pl.multiple_of((2 * p + c) * rank_kv, rank_kv), rank_kv)
    qraw[pl.ds(pl.multiple_of(t * rank_q, rank_q), rank_q), :] = raw[0:rank_q].astype(BF)
    kvraw[kv_at(chip, core), :] = raw[rank_q:rank_q + rank_kv].astype(BF)
    raw_ring = Gather(nx, chip, along_x,
                      [lambda p, c: kvraw.at[kv_at(p, c), :], lambda p, c: qraw.at[q_at(p, c, 0), :], lambda p, c: qraw.at[q_at(p, c, 1), :]],
                      raw_x, partner, core)
    raw_ring.start()
    kv[z, 2 * PLAIN:KROWS, :] = axial_turn(raw[rank_q + rank_kv:], *turn).astype(BF)

    for s in range(1, raw_ring.reach + 1):
        raw_ring.step(s)
        if steps_z:
            ctx_step(steps_z.pop(0))
    for s in range(0, raw_ring.reach + 1):
        raw_ring.pair_step(s)

    ckv = rms_columns(kvraw[...], kv_gain)
    own = jnp.dot(ukvT[...], ckv, preferred_element_type=F32).astype(BF)
    kv[z, 0:2 * PLAIN, :] = own[0:2 * PLAIN]
    kv[z, KROWS:KROWS + VROWS, :] = own[2 * PLAIN:]
    kv_half = (KROWS + VROWS) // 2
    kv_ring = Gather(nz, z, along_z, [lambda p, c: kv.at[p, pl.ds(0, kv_half)], lambda p, c: kv.at[p, pl.ds(kv_half, kv_half)]], kv_z)
    while steps_z:
        ctx_step(steps_z.pop(0))
    kv_ring.start()

    cq = rms_columns(qraw[...], q_gain)
    q = jnp.dot(uqT[...], cq, preferred_element_type=F32)
    per = PLAIN + ROTARY
    for head in range(2):
        mine = q[head * per:(head + 1) * per]
        plain = mine[0:PLAIN].astype(BF)
        blank = jnp.zeros_like(plain)
        qb[head, head * PLAIN:(head + 1) * PLAIN, :] = plain
        qb[head, (1 - head) * PLAIN:(2 - head) * PLAIN, :] = blank
        qb[head, 2 * PLAIN:KROWS, :] = axial_turn(mine[PLAIN:], *turn).astype(BF)
    m_ref[...] = jnp.full_like(m_ref, NEGATIVE)
    l_ref[...] = jnp.zeros_like(l_ref)
    acc[...] = jnp.zeros_like(acc)

    def attend(keysT, valuesT, biased):
        keys = keysT.astype(F32).T.astype(BF)
        for head in range(2):
            s = jnp.dot(keys, qb[head], preferred_element_type=F32) * (SCORE * LOG2E)
            if biased:
                s = s + bias_ref[0, head] * LOG2E
            old = m_ref[head]
            new = jnp.maximum(old, jnp.max(s, axis=0, keepdims=True))
            alpha = jnp.exp2(old - new)
            e = jnp.exp2(s - new)
            m_ref[head] = new
            l_ref[head] = l_ref[head] * alpha + jnp.sum(e, axis=0, keepdims=True)
            acc[head] = acc[head] * alpha + jnp.dot(valuesT[head * VALUE:(head + 1) * VALUE], e.astype(BF), preferred_element_type=F32)

    for s in range(1, ctx_ring.reach + 1):
        ctx_ring.pair_step(s)

    @pl.loop(0, nz)
    def _(i):
        at = pl.ds(pl.multiple_of(i * crows, crows), crows)
        hc[at, :] = modulated(ctx[i], mod[1:2, :], mod[3:4, :])

    rawc = jnp.dot(hc[...], wcat[...], preferred_element_type=F32).T
    kvcraw[kv_at(chip, core), :] = rawc[rank_q:rank_q + rank_kv].astype(BF)
    chalf = kvcraw.shape[1] // 2
    rawc_ring = Gather(nx, chip, along_x,
                       [lambda p, c: kvcraw.at[kv_at(p, c), pl.ds(0, chalf)], lambda p, c: kvcraw.at[kv_at(p, c), pl.ds(chalf, chalf)]],
                       rawc_x, partner, core)
    rawc_ring.start()
    kvc[2 * PLAIN:KROWS, :] = rawc[rank_q + rank_kv:].astype(BF)

    attend(kv[z, 0:KROWS, :], kv[z, KROWS:KROWS + VROWS, :], False)
    reach = kv_ring.reach

    def ring_source(d, s):
        return lax.rem(z + jnp.where(d == 0, nz - s, s), nz)

    def arrive(d, s, ch):
        piece = kv.at[ring_source(d, s), pl.ds(ch * kv_half, kv_half)]
        return pltpu.make_async_remote_copy(piece, piece, kv_z[1].at[d, s, ch], kv_z[0].at[d, s, ch],
                                            device_id=along_z(jnp.where(d == 0, nz - 1, 1)), device_id_type=MESH)

    def forward(d, s, ch):
        piece = kv.at[ring_source(d, s), pl.ds(ch * kv_half, kv_half)]
        return pltpu.make_async_remote_copy(piece, piece, kv_z[1].at[d, s, ch], kv_z[0].at[d, s + 1, ch],
                                            device_id=along_z(jnp.where(d == 0, 1, nz - 1)), device_id_type=MESH)

    def take(k, waits_only_last):
        s = (k + 1) // 2
        d = 1 - lax.rem(k, 2)
        if waits_only_last:
            kv_ring.ring_arrival(0, reach, 0).wait_recv()
            kv_ring.ring_arrival(1, reach, 1).wait_recv()
        else:
            for ch in range(2):
                arrive(d, s, ch).wait_recv()

                @pl.when((s + 1 < reach) | ((s + 1 == reach) & (d == ch)))
                def _():
                    forward(d, s, ch).start()
        b = ring_source(d, s)
        attend(kv[b, 0:KROWS, :], kv[b, KROWS:KROWS + VROWS, :], False)

    split = min(2 * reach - 1, 2 * rawc_ring.reach + 1)

    def early(k, carry):
        take(k, False)
        return carry

    for s in range(1, rawc_ring.reach + 1):
        rawc_ring.step(s)
    for s in range(0, rawc_ring.reach + 1):
        rawc_ring.pair_step(s)
    lax.fori_loop(1, 2 * reach - 1, early, 0)
    ckvc = rms_columns(kvcraw[...], kv_gain)
    ownc = jnp.dot(ukvT[...], ckvc, preferred_element_type=F32).astype(BF)
    kvc[0:2 * PLAIN, :] = ownc[0:2 * PLAIN]
    kvc[KROWS:KROWS + VROWS, :] = ownc[2 * PLAIN:]
    attend(kvc[0:KROWS, :], kvc[KROWS:KROWS + VROWS, :], True)
    take(2 * reach - 1, True)

    outT = jnp.concatenate([acc[0] / l_ref[0], acc[1] / l_ref[1]], axis=0)
    mine_at = lambda p, c: pl.ds(pl.multiple_of((2 * p + c) * VROWS, VROWS), VROWS)
    att[:, mine_at(chip, core)] = outT.T.astype(BF)
    thalf = tok // 2
    att_ring = Gather(nx, chip, along_x,
                      [lambda p, c: att.at[pl.ds(0, thalf), mine_at(p, c)], lambda p, c: att.at[pl.ds(thalf, thalf), mine_at(p, c)]],
                      att_x, partner, core)
    att_ring.start()
    for s in range(1, att_ring.reach + 1):
        att_ring.step(s)

    def am(k, incoming):
        far = lax.rem(t + nt - k, nt) if incoming else lax.rem(t + k, nt)
        if incoming:
            return pltpu.make_async_remote_copy(pbuf.at[far], mbuf.at[far], a_s.at[k], a_r.at[k], device_id={"tp": far}, device_id_type=MESH)
        return pltpu.make_async_remote_copy(pbuf.at[far], mbuf.at[t], a_s.at[k], a_r.at[k], device_id={"tp": far}, device_id_type=MESH)

    for s in range(0, att_ring.reach + 1):
        att_ring.pair_step(s)
    proj = jnp.dot(att[...], wo[...], preferred_element_type=F32)
    for j in range(nt):
        pbuf[j] = proj[j * rows:(j + 1) * rows].astype(BF)
    for k in sorted(range(1, nt), key=lambda k: -min(k, nt - k)):
        am(k, False).start()
    mbuf[t] = pbuf[t]
    for k in range(1, nt):
        am(k, True).wait_recv()
    for j in range(nt):
        cut = slice(j * part, (j + 1) * part)
        out_ref[:, cut] = (own_lat[:, cut].astype(F32) + mod[4:5, cut] * mbuf[j].astype(F32)).astype(BF)

    for k in range(1, nz):
        zm(k, False).wait_send()
    for k in range(1, nt):
        xm(k, False).wait_send()
        am(k, False).wait_send()
    lat_ring.finish()
    for s in range(ctx_ring.reach + 1):
        for ch in range(2):
            for d in range(2):
                if ctx_ring.active(d, s + 1, ch):
                    ctx_ring.ring_copy(d, s, ch).wait_send()
                if s > 0 and ctx_ring.active(d, s, ch):
                    ctx_ring.pair_copy(d, s, ch, core).wait_send()
    raw_ring.finish()
    rawc_ring.finish()
    kv_ring.finish()
    att_ring.finish()


def sems(count, chunks, paired):
    kinds = 4 if paired else 2
    return tuple(pltpu.SemaphoreType.DMA((2, count // 2 + 2, chunks)) for _ in range(kinds))


def on_device(latents, conditions, context, w_shift, w_scale, w_gate, w_qdown, w_kvdown, w_rope, q_gain,
              latent_norm_gain, query_up_weight, key_up_weight, value_up_weight, context_bias, w_out):
    nz, nt = lax.axis_size("sp"), lax.axis_size("tp")
    nx = nt // 2
    rows, width = latents.shape
    tok = rows * nt
    crows = context.shape[0]
    rank_q, rank_kv = w_qdown.shape[1], w_kvdown.shape[1]
    part = width // nt
    vm = pltpu.VMEM
    dma = pltpu.SemaphoreType.DMA
    scratch = [
        vm((nt, rows, width), BF), vm((nz, crows, width), BF), vm((rows, width), BF),
        vm(w_qdown.shape, BF), vm(w_kvdown.shape, BF), vm(w_rope.shape, BF), vm(query_up_weight.shape, BF),
        vm(key_up_weight.shape, BF), vm(value_up_weight.shape, BF), vm(w_out.shape, BF),
        vm((width, rank_q + rank_kv + ROTARY), BF), vm(query_up_weight.shape[::-1], BF), vm((2 * PLAIN + VROWS, nt * rank_kv), BF),
        vm((nz, 8, part), F32), vm((nt, 8, part), F32), vm((8, width), F32),
        vm((tok, width), BF), vm((nz * crows, width), BF),
        vm((nt * rank_q, tok), BF), vm((nt * rank_kv, tok), BF), vm((nt * rank_kv, nz * crows), BF),
        vm((nz, KROWS + VROWS, tok), BF), vm((KROWS + VROWS, nz * crows), BF), vm((2, KROWS, tok), BF),
        vm((2, 1, tok), F32), vm((2, 1, tok), F32), vm((2, VALUE, tok), F32),
        vm((tok, nt * VROWS), BF), vm((nt, rows, part), BF), vm((nt, rows, part), BF),
        dma((10,)), dma((nz,)), dma((nz,)), dma((nt,)), dma((nt,)), dma((nt,)), dma((nt,)),
        sems(nx, 2, True), sems(nz, 2, True), sems(nx, 3, True), sems(nx, 2, True), sems(nz, 2, False), sems(nx, 2, True),
    ]
    here = pl.BlockSpec(memory_space=vm)
    away = pl.BlockSpec(memory_space=pl.ANY)
    small = pl.BlockSpec(memory_space=pltpu.SMEM)
    return pl.pallas_call(
        functools.partial(kernel, nz, nt),
        out_shape=jax.ShapeDtypeStruct((rows, width), BF),
        in_specs=[away, here, away, here, here, here, away, away, away, here, here, away, away, away, small, away],
        out_specs=here,
        scratch_shapes=scratch,
        compiler_params=pltpu.CompilerParams(collective_id=0, has_side_effects=True, vmem_limit_bytes=60 * 1024 * 1024),
        name="block",
    )(latents, conditions, context, w_shift, w_scale, w_gate, w_qdown, w_kvdown, w_rope, q_gain.reshape(1, -1),
      latent_norm_gain.reshape(1, -1), query_up_weight, key_up_weight, value_up_weight, context_bias.reshape(1, -1), w_out)


def solution(mesh):
    in_specs = (
        P(("grp", "sp", "tp"), None),
        P("grp", "sp"),
        P(("grp", "sp"), None),
        P("sp", "tp"),
        P("sp", "tp"),
        P("sp", "tp"),
        P(None, "tp"),
        P(None, "tp"),
        P(),
        P(),
        P(),
        P(None, "tp"),
        P(None, "tp"),
        P(None, "tp"),
        P("tp"),
        P(None, "tp"),
    )
    return jax.shard_map(on_device, mesh=mesh, in_specs=in_specs, out_specs=P(("grp", "sp", "tp"), None), check_vma=False)
```

time: 377 us -> 203 us (0.54)
  Pallas kernels: 0 us -> 195 us
  waiting for transfers between devices: 114 us -> 0 us
  blocking collectives: 102 us -> 0 us
  starting transfers between devices: 44.4 us -> 0 us
  matrix products: 42.6 us -> 0 us
  local copies, waits for them, and re-layouts: 41.9 us -> 7.71 us
  other arithmetic: 14.3 us -> 0 us
  between operations: 13.5 us -> 0.01 us
    pallas_call x0 -> x1, Pallas kernels: none -> 195 us  [on_device(): pl.pallas_call(functools.partial(kernel, nz, nt), out_shape=jax.ShapeDtyp...]
    all_gather x3 -> x0, waiting for transfers between devices: 107 us -> none  [the longest x1 49.6 us: in_one_piece(): lax.all_gather(both, axis, axis=dim, tiled=True)]
    all_gather x5 -> x0, blocking collectives: 87.4 us -> none  [the longest x1 21.9 us: on_device(): modulation = lax.all_gather(summed, 'tp', axis=1, tiled=True)]
    all_to_all x1 -> x0, starting transfers between devices: 44.2 us -> none  [sent_to_all(): lax.all_to_all(jnp.broadcast_to(shard[None], (peers, *shard.shape)), axis...]
    dot_general x58 -> x0, matrix products: 42.6 us -> none  [the longest x16 17.9 us: attend_block(): jnp.einsum('ihd,jd->ihj', q_rope, rope_block, preferred_element_type=jnp....]
    dynamic_slice x48 -> x0, local copies, waits for them, and re-layouts: 19.1 us -> none  [on_device(): result, unused = lax.scan(step_fn, initial, stacked)]
    all_to_all x1 -> x0, blocking collectives: 14.9 us -> none  [on_device(): lax.all_to_all(proj_cols.astype(jnp.bfloat16), 'tp', split_axis=0, concat...]
    reduce_sum x24 -> x0, other arithmetic: 7.8 us -> none  [the longest x16 3.06 us: attend_block(): running_sum = running_sum * rescale + jnp.sum(exponent, axis=-1)]
  transfers between devices with their start and end apart: 4 -> 0, of which waited for: 4 -> 0; matrix products, arithmetic and copies ran while one was open for 3% -> 0% of each run, Pallas kernels for 0% -> 0%
where the time goes in v1:
time: 203 us
  Pallas kernels  195 us (96%)
  local copies, waits for them, and re-layouts  7.71 us (4%)
    pallas_call x1, Pallas kernels, on_device(): pl.pallas_call(functools.partial(kernel, nz, nt), out_shape=jax.ShapeDtyp...  195 us
    unnamed x11, local copies, waits for them, and re-layouts  7.71 us

profile of v1, /device:TPU:65, one launch (start us, length us, event | category | flops | bytes accessed | tf_op | source)
XLA Modules:
  0.0 202.7 jit_solution(13992256779752312962)
XLA Ops:
  0.0 0.0 copy-start
  0.0 2.1 %copy.20.refs_11_ = bf16[1024,192]{1,0:T(8,128)(2,1)} copy(bf16[1024,192]{0,1:T(8,128)(2,1)} %param.27) | data formatting | bytes 786432 | tf_op args[11]
  2.1 0.0 copy-done
  2.1 0.0 copy-start.1
  2.1 1.3 copy.17.refs_6_
  3.4 0.0 copy-done.1
  3.4 0.0 copy-start.2
  3.4 1.4 copy.18.refs_7_
  4.7 0.0 copy-done.2
  4.7 1.3 copy.19.refs_8_
  6.1 195.0 %block.1 = bf16[24,4096]{1,0:T(8,128)(2,1)} custom-call(bf16[24,4096]{1,0:T(8,128)(2,1)} %refs_0_.1, f32[2,256]{1,0:T(2,128)} %refs_1_.1, bf16[32,4096]{1,0:T(8,128)(2,1)} %refs_2_.1, bf16[256,256]{1,0:T(8,128)(2,1)} %refs_3_.1, bf16[256,256]{1,0:T(8,128)(2,1)} %refs_4_.1, bf16[256,256]{1,0:T(8,128)(2,1)} %refs_5_.1, bf16[4096,64]{1,0:T(8,128)(2,1)} %copy.17.refs_6_, ...), custom_call_target="tpu_custom_call" | custom-call | tf_op jit(solution)/shard_map/block/pallas_call | solution.py:460
  201.1 1.6 copy.22
Async XLA Ops:
  0.0 2.1 %copy-start = (bf16[4096,64]{0,1:T(8,128)(2,1)S(1)}, bf16[4096,64]{0,1:T(8,128)(2,1)}, u32[]{:S(2)}) copy-start(bf16[4096,64]{0,1:T(8,128)(2,1)} %param.22) | copy-start | bytes 1572868
  2.1 1.3 copy-start.1
  3.4 1.4 copy-start.2

commit v2 on v1

--- a/solution.py
+++ b/solution.py
@@ -117,21 +117,21 @@
 
 def kernel(nz, nt, *refs):
     (lat_hbm, cond_ref, ctx_hbm, wsh_ref, wsc_ref, wg_ref, wq_hbm, wkv_hbm, wr_hbm, qg_ref, kg_ref,
-     uq_hbm, uk_hbm, uv_hbm, bias_ref, wo_hbm, out_ref,
-     lat, ctx, own_lat, wq, wkv, wr, uq, uk, uv, wo,
+     uq_hbm, uk_hbm, uv_hbm, bias_ref, wo_hbm, proj_ref, gate_ref,
+     lat, ctx, mean_ref, rstd_ref, uk, uv, wo,
      wcat, uqT, ukvT, zmod, xmod, mod, h, hc, qraw, kvraw, kvcraw, kv, kvc, qb,
-     m_ref, l_ref, acc, att, pbuf, mbuf,
+     m_ref, l_ref, acc, att, pbuf, mbuf, q_gain_ref, kv_gain_ref,
      load_sem, zm_s, zm_r, xm_s, xm_r, a_s, a_r, lat_x, ctx_z, raw_x, rawc_x, kv_z, att_x) = refs
     z, t = lax.axis_index("sp"), lax.axis_index("tp")
     core = lax.rem(t, 2)
     chip = t // 2
     nx = nt // 2
-    rows = own_lat.shape[0]
+    rows = lat.shape[1]
     tok = rows * nt
     crows = ctx.shape[1]
-    width = own_lat.shape[1]
+    width = lat.shape[2]
     part = width // nt
-    rank_q, rank_kv = wq.shape[1], wkv.shape[1]
+    rank_q, rank_kv = wq_hbm.shape[0], wkv_hbm.shape[0]
     along_z = lambda k: {"sp": lax.rem(z + k, nz)}
     along_x = lambda k: {"tp": lax.rem(t + 2 * k, nt)}
     partner = {"tp": t + 1 - 2 * core}
@@ -140,14 +140,13 @@
     loads = [
         pltpu.make_async_copy(lat_hbm, lat.at[t], load_sem.at[0]),
         pltpu.make_async_copy(ctx_hbm, ctx.at[z], load_sem.at[1]),
-        pltpu.make_async_copy(lat_hbm, own_lat, load_sem.at[2]),
-        pltpu.make_async_copy(wq_hbm, wq, load_sem.at[3]),
-        pltpu.make_async_copy(wkv_hbm, wkv, load_sem.at[4]),
-        pltpu.make_async_copy(wr_hbm, wr, load_sem.at[5]),
-        pltpu.make_async_copy(uq_hbm, uq, load_sem.at[6]),
-        pltpu.make_async_copy(uk_hbm, uk, load_sem.at[7]),
-        pltpu.make_async_copy(uv_hbm, uv, load_sem.at[8]),
-        pltpu.make_async_copy(wo_hbm, wo, load_sem.at[9]),
+        pltpu.make_async_copy(wq_hbm, wcat.at[pl.ds(0, rank_q)], load_sem.at[2]),
+        pltpu.make_async_copy(wkv_hbm, wcat.at[pl.ds(rank_q, rank_kv)], load_sem.at[3]),
+        pltpu.make_async_copy(wr_hbm, wcat.at[pl.ds(rank_q + rank_kv, ROTARY)], load_sem.at[4]),
+        pltpu.make_async_copy(uq_hbm, uqT, load_sem.at[5]),
+        pltpu.make_async_copy(uk_hbm, uk, load_sem.at[6]),
+        pltpu.make_async_copy(uv_hbm, uv, load_sem.at[7]),
+        pltpu.make_async_copy(wo_hbm, wo, load_sem.at[8]),
     ]
     barrier = pltpu.get_barrier_semaphore()
     for k in range(1, nz):
@@ -198,22 +197,42 @@
 
     for load in loads[2:]:
         load.wait()
-    steps = 8
-    depth = width // steps
-    for i in range(steps):
-        cut = pl.ds(i * depth, depth)
-        wcat[cut, :] = jnp.concatenate([wq[cut, :], wkv[cut, :], wr[cut, :]], axis=1)
-    uqT[...] = uq[...].astype(F32).T.astype(BF)
     ukvT[0:2 * PLAIN, :] = uk[...].astype(F32).T.astype(BF)
     ukvT[2 * PLAIN:2 * PLAIN + VROWS, :] = uv[...].astype(F32).T.astype(BF)
-    q_gain = jnp.broadcast_to(qg_ref[...], (8, qg_ref.shape[1])).T[:, 0:1]
-    kv_gain = jnp.broadcast_to(kg_ref[...], (8, kg_ref.shape[1])).T[:, 0:1]
+    q_gain_ref[...] = jnp.broadcast_to(qg_ref[...], (8, qg_ref.shape[1])).T[:, 0:1]
+    kv_gain_ref[...] = jnp.broadcast_to(kg_ref[...], (8, kg_ref.shape[1])).T[:, 0:1]
     pos = lax.broadcasted_iota(jnp.int32, (8, tok), 1) + z * tok
     freq = jnp.exp(lax.broadcasted_iota(jnp.int32, (8, tok), 0).astype(F32) * (-math.log(10000.0) / 8))
     row_angle = (pos >> 6).astype(F32) * freq
     col_angle = (pos & (GRID_W - 1)).astype(F32) * freq
     turn = (jnp.cos(row_angle), jnp.sin(row_angle), jnp.cos(col_angle), jnp.sin(col_angle))
 
+    def ctx_step(s):
+        for ch in range(2):
+            for d in range(2):
+                if ctx_ring.active(d, s, ch):
+                    ctx_ring.ring_arrival(d, s, ch).wait_recv()
+                    if ctx_ring.active(d, s + 1, ch):
+                        ctx_ring.ring_copy(d, s, ch).start()
+                    ctx_ring.pair_copy(d, s, ch, core).start()
+
+    steps_z = list(range(1, ctx_ring.reach + 1))
+
+    def ctx_next(least=0):
+        if len(steps_z) > least:
+            ctx_step(steps_z.pop(0))
+
+    def chip_rows(p):
+        return jnp.concatenate([lat[2 * p].astype(F32), lat[2 * p + 1].astype(F32)], axis=0)
+
+    def note_statistics(p):
+        values = chip_rows(p)
+        center = values - jnp.mean(values, axis=-1, keepdims=True)
+        mean_ref[p] = jnp.mean(values, axis=-1, keepdims=True)
+        rstd_ref[p] = lax.rsqrt(jnp.mean(center * center, axis=-1, keepdims=True) + EPSILON)
+
+    lat_ring.step(1)
+    ctx_next()
     for k in reversed(order):
         zm(k, True).wait_recv()
     total = zmod[0]
@@ -222,36 +241,38 @@
     xmod[t] = total
     for k in range(1, nt):
         xm(k, False).start()
-
-    def ctx_step(s):
-        for ch in range(2):
-            for d in range(2):
-                if ctx_ring.active(d, s, ch):
-                    ctx_ring.ring_arrival(d, s, ch).wait_recv()
-                    if ctx_ring.active(d, s + 1, ch):
-                        ctx_ring.ring_copy(d, s, ch).start()
-                    ctx_ring.pair_copy(d, s, ch, core).start()
-
-    steps_z = list(range(1, ctx_ring.reach + 1))
-    for s in range(1, lat_ring.reach + 1):
+    far = lat_ring.reach
+    for s in range(2, far + 1):
+        lat_ring.pair_step(s - 2)
+
+        @pl.loop(0, 1 if s == 2 else 2)
+        def _(i):
+            note_statistics(lax.rem(chip + jnp.where(i == 0, nx - (s - 2), s - 2), nx))
+
         lat_ring.step(s)
-        for _ in range(1):
-            if steps_z:
-                ctx_step(steps_z.pop(0))
-    for s in range(0, lat_ring.reach + 1):
-        lat_ring.pair_step(s)
+        ctx_next()
+    lat_ring.pair_step(far - 1)
+
+    @pl.loop(0, 2 if far > 1 else 1)
+    def _(i):
+        note_statistics(lax.rem(chip + jnp.where(i == 0, nx - (far - 1), far - 1), nx))
+
+    lat_ring.pair_step(far)
+    note_statistics(lax.rem(chip + far, nx))
     for k in range(1, nt):
         xm(k, True).wait_recv()
     for j in range(nt):
         mod[:, j * part:(j + 1) * part] = xmod[j]
 
-    @pl.loop(0, nt // 2)
-    def _(i):
-        block = jnp.concatenate([lat[2 * i].astype(F32), lat[2 * i + 1].astype(F32)], axis=0)
-        at = pl.ds(pl.multiple_of(i * 2 * rows, 2 * rows), 2 * rows)
-        h[at, :] = modulated(block, mod[0:1, :], mod[2:3, :])
-
-    raw = jnp.dot(h[...], wcat[...], preferred_element_type=F32).T
+    for piece in range(2):
+        @pl.loop(piece * nx // 2, (piece + 1) * nx // 2)
+        def _(p):
+            at = pl.ds(pl.multiple_of(p * 2 * rows, 2 * rows), 2 * rows)
+            normed = (chip_rows(p) - mean_ref[p]) * rstd_ref[p]
+            h[at, :] = (normed * (1.0 + mod[2:3, :]) + mod[0:1, :]).astype(BF)
+        ctx_next()
+
+    raw = lax.dot_general(h[...], wcat[...], (((1,), (1,)), ((), ())), preferred_element_type=F32).T
     q_at = lambda p, c, i: pl.ds(pl.multiple_of((2 * p + c) * rank_q + i * (rank_q // 2), rank_q // 2), rank_q // 2)
     kv_at = lambda p, c: pl.ds(pl.multiple_of((2 * p + c) * rank_kv, rank_kv), rank_kv)
     qraw[pl.ds(pl.multiple_of(t * rank_q, rank_q), rank_q), :] = raw[0:rank_q].astype(BF)
@@ -264,22 +285,22 @@
 
     for s in range(1, raw_ring.reach + 1):
         raw_ring.step(s)
-        if steps_z:
-            ctx_step(steps_z.pop(0))
+        if s == 2:
+            ctx_next(1)
     for s in range(0, raw_ring.reach + 1):
         raw_ring.pair_step(s)
 
-    ckv = rms_columns(kvraw[...], kv_gain)
+    ckv = rms_columns(kvraw[...], kv_gain_ref[...])
     own = jnp.dot(ukvT[...], ckv, preferred_element_type=F32).astype(BF)
     kv[z, 0:2 * PLAIN, :] = own[0:2 * PLAIN]
     kv[z, KROWS:KROWS + VROWS, :] = own[2 * PLAIN:]
     kv_half = (KROWS + VROWS) // 2
     kv_ring = Gather(nz, z, along_z, [lambda p, c: kv.at[p, pl.ds(0, kv_half)], lambda p, c: kv.at[p, pl.ds(kv_half, kv_half)]], kv_z)
-    while steps_z:
-        ctx_step(steps_z.pop(0))
     kv_ring.start()
-
-    cq = rms_columns(qraw[...], q_gain)
+    while len(steps_z) > 1:
+        ctx_next()
+
+    cq = rms_columns(qraw[...], q_gain_ref[...])
     q = jnp.dot(uqT[...], cq, preferred_element_type=F32)
     per = PLAIN + ROTARY
     for head in range(2):
@@ -307,79 +328,107 @@
             l_ref[head] = l_ref[head] * alpha + jnp.sum(e, axis=0, keepdims=True)
             acc[head] = acc[head] * alpha + jnp.dot(valuesT[head * VALUE:(head + 1) * VALUE], e.astype(BF), preferred_element_type=F32)
 
+    attend(kv[z, 0:KROWS, :], kv[z, KROWS:KROWS + VROWS, :], False)
+    while steps_z:
+        ctx_next()
     for s in range(1, ctx_ring.reach + 1):
         ctx_ring.pair_step(s)
-
-    @pl.loop(0, nz)
-    def _(i):
-        at = pl.ds(pl.multiple_of(i * crows, crows), crows)
-        hc[at, :] = modulated(ctx[i], mod[1:2, :], mod[3:4, :])
-
-    rawc = jnp.dot(hc[...], wcat[...], preferred_element_type=F32).T
-    kvcraw[kv_at(chip, core), :] = rawc[rank_q:rank_q + rank_kv].astype(BF)
     chalf = kvcraw.shape[1] // 2
     rawc_ring = Gather(nx, chip, along_x,
                        [lambda p, c: kvcraw.at[kv_at(p, c), pl.ds(0, chalf)], lambda p, c: kvcraw.at[kv_at(p, c), pl.ds(chalf, chalf)]],
                        rawc_x, partner, core)
-    rawc_ring.start()
-    kvc[2 * PLAIN:KROWS, :] = rawc[rank_q + rank_kv:].astype(BF)
-
-    attend(kv[z, 0:KROWS, :], kv[z, KROWS:KROWS + VROWS, :], False)
     reach = kv_ring.reach
 
     def ring_source(d, s):
         return lax.rem(z + jnp.where(d == 0, nz - s, s), nz)
 
-    def arrive(d, s, ch):
+    def hop(d, s, ch, into):
         piece = kv.at[ring_source(d, s), pl.ds(ch * kv_half, kv_half)]
-        return pltpu.make_async_remote_copy(piece, piece, kv_z[1].at[d, s, ch], kv_z[0].at[d, s, ch],
-                                            device_id=along_z(jnp.where(d == 0, nz - 1, 1)), device_id_type=MESH)
-
-    def forward(d, s, ch):
-        piece = kv.at[ring_source(d, s), pl.ds(ch * kv_half, kv_half)]
-        return pltpu.make_async_remote_copy(piece, piece, kv_z[1].at[d, s, ch], kv_z[0].at[d, s + 1, ch],
-                                            device_id=along_z(jnp.where(d == 0, 1, nz - 1)), device_id_type=MESH)
-
-    def take(k, waits_only_last):
-        s = (k + 1) // 2
-        d = 1 - lax.rem(k, 2)
-        if waits_only_last:
-            kv_ring.ring_arrival(0, reach, 0).wait_recv()
-            kv_ring.ring_arrival(1, reach, 1).wait_recv()
-        else:
-            for ch in range(2):
-                arrive(d, s, ch).wait_recv()
-
-                @pl.when((s + 1 < reach) | ((s + 1 == reach) & (d == ch)))
+        return pltpu.make_async_remote_copy(piece, piece, kv_z[1].at[d, s, ch], kv_z[0].at[d, into, ch],
+                                            device_id=along_z(1 if d == 0 else nz - 1), device_id_type=MESH)
+
+    def pass_on(s, ch):
+        for d in range(2):
+            hop(d, s, ch, s).wait_recv()
+        for d in range(2):
+            if d == ch:
+                hop(d, s, ch, s + 1).start()
+            else:
+                @pl.when(s + 1 < reach)
                 def _():
-                    forward(d, s, ch).start()
+                    hop(d, s, ch, s + 1).start()
+
+    def attend_block(d, s):
         b = ring_source(d, s)
         attend(kv[b, 0:KROWS, :], kv[b, KROWS:KROWS + VROWS, :], False)
 
-    split = min(2 * reach - 1, 2 * rawc_ring.reach + 1)
-
-    def early(k, carry):
-        take(k, False)
+    def context_quarter(quarter):
+        @pl.loop(quarter * nz // 4, (quarter + 1) * nz // 4)
+        def _(i):
+            at = pl.ds(pl.multiple_of(i * crows, crows), crows)
+            hc[at, :] = modulated(ctx[i], mod[1:2, :], mod[3:4, :])
+
+    def context_down():
+        rawc = lax.dot_general(hc[...], wcat[...], (((1,), (1,)), ((), ())), preferred_element_type=F32).T
+        kvcraw[kv_at(chip, core), :] = rawc[rank_q:rank_q + rank_kv].astype(BF)
+        kvc[2 * PLAIN:KROWS, :] = rawc[rank_q + rank_kv:].astype(BF)
+        rawc_ring.start()
+
+    def context_up():
+        for s in range(0, rawc_ring.reach + 1):
+            rawc_ring.pair_step(s)
+        ckvc = rms_columns(kvcraw[...], kv_gain_ref[...])
+        ownc = jnp.dot(ukvT[...], ckvc, preferred_element_type=F32).astype(BF)
+        kvc[0:2 * PLAIN, :] = ownc[0:2 * PLAIN]
+        kvc[KROWS:KROWS + VROWS, :] = ownc[2 * PLAIN:]
+
+    jobs = [functools.partial(context_quarter, i) for i in range(4)] + [context_down]
+    jobs += [functools.partial(rawc_ring.step, s) for s in range(1, rawc_ring.reach + 1)] + [context_up]
+    slots = 2 * (reach - 1)
+    place = {}
+    for i, job in enumerate(jobs):
+        spare = i if i < 5 else 5 + 2 * (i - 5) + 1
+        place.setdefault(min(spare, slots - 1), []).append(job)
+
+    def do_jobs(slot, now):
+        for at, work in place.items():
+            if at % 2 == slot:
+                @pl.when(now == at // 2 + 1)
+                def _():
+                    for job in work:
+                        job()
+
+    def kv_step(s, carry):
+        pass_on(s, 0)
+
+        @pl.when(s > 1)
+        def _():
+            attend_block(0, s - 1)
+        do_jobs(0, s)
+        pass_on(s, 1)
+
+        @pl.when(s > 1)
+        def _():
+            attend_block(1, s - 1)
+        do_jobs(1, s)
         return carry
 
-    for s in range(1, rawc_ring.reach + 1):
-        rawc_ring.step(s)
-    for s in range(0, rawc_ring.reach + 1):
-        rawc_ring.pair_step(s)
-    lax.fori_loop(1, 2 * reach - 1, early, 0)
-    ckvc = rms_columns(kvcraw[...], kv_gain)
-    ownc = jnp.dot(ukvT[...], ckvc, preferred_element_type=F32).astype(BF)
-    kvc[0:2 * PLAIN, :] = ownc[0:2 * PLAIN]
-    kvc[KROWS:KROWS + VROWS, :] = ownc[2 * PLAIN:]
+    lax.fori_loop(1, reach, kv_step, 0)
+
+    @pl.loop(0, 2)
+    def _(d):
+        attend_block(d, reach - 1)
     attend(kvc[0:KROWS, :], kvc[KROWS:KROWS + VROWS, :], True)
-    take(2 * reach - 1, True)
+    kv_ring.ring_arrival(0, reach, 0).wait_recv()
+    kv_ring.ring_arrival(1, reach, 1).wait_recv()
+    attend_block(0, reach)
 
     outT = jnp.concatenate([acc[0] / l_ref[0], acc[1] / l_ref[1]], axis=0)
     mine_at = lambda p, c: pl.ds(pl.multiple_of((2 * p + c) * VROWS, VROWS), VROWS)
     att[:, mine_at(chip, core)] = outT.T.astype(BF)
-    thalf = tok // 2
+    fourth = tok // 4
     att_ring = Gather(nx, chip, along_x,
-                      [lambda p, c: att.at[pl.ds(0, thalf), mine_at(p, c)], lambda p, c: att.at[pl.ds(thalf, thalf), mine_at(p, c)]],
+                      [lambda p, c, i=i: att.at[pl.ds(i * fourth, fourth), mine_at(p, c)] for i in range(4)],
                       att_x, partner, core)
     att_ring.start()
     for s in range(1, att_ring.reach + 1):
@@ -399,11 +448,12 @@
     for k in sorted(range(1, nt), key=lambda k: -min(k, nt - k)):
         am(k, False).start()
     mbuf[t] = pbuf[t]
+    gate_ref[...] = mod[4:5, :]
     for k in range(1, nt):
         am(k, True).wait_recv()
     for j in range(nt):
         cut = slice(j * part, (j + 1) * part)
-        out_ref[:, cut] = (own_lat[:, cut].astype(F32) + mod[4:5, cut] * mbuf[j].astype(F32)).astype(BF)
+        proj_ref[:, cut] = mbuf[j]
 
     for k in range(1, nz):
         zm(k, False).wait_send()
@@ -441,32 +491,33 @@
     vm = pltpu.VMEM
     dma = pltpu.SemaphoreType.DMA
     scratch = [
-        vm((nt, rows, width), BF), vm((nz, crows, width), BF), vm((rows, width), BF),
-        vm(w_qdown.shape, BF), vm(w_kvdown.shape, BF), vm(w_rope.shape, BF), vm(query_up_weight.shape, BF),
+        vm((nt, rows, width), BF), vm((nz, crows, width), BF), vm((nx, 2 * rows, 1), F32), vm((nx, 2 * rows, 1), F32),
         vm(key_up_weight.shape, BF), vm(value_up_weight.shape, BF), vm(w_out.shape, BF),
-        vm((width, rank_q + rank_kv + ROTARY), BF), vm(query_up_weight.shape[::-1], BF), vm((2 * PLAIN + VROWS, nt * rank_kv), BF),
+        vm((rank_q + rank_kv + ROTARY, width), BF), vm(query_up_weight.shape[::-1], BF), vm((2 * PLAIN + VROWS, nt * rank_kv), BF),
         vm((nz, 8, part), F32), vm((nt, 8, part), F32), vm((8, width), F32),
         vm((tok, width), BF), vm((nz * crows, width), BF),
         vm((nt * rank_q, tok), BF), vm((nt * rank_kv, tok), BF), vm((nt * rank_kv, nz * crows), BF),
         vm((nz, KROWS + VROWS, tok), BF), vm((KROWS + VROWS, nz * crows), BF), vm((2, KROWS, tok), BF),
         vm((2, 1, tok), F32), vm((2, 1, tok), F32), vm((2, VALUE, tok), F32),
         vm((tok, nt * VROWS), BF), vm((nt, rows, part), BF), vm((nt, rows, part), BF),
-        dma((10,)), dma((nz,)), dma((nz,)), dma((nt,)), dma((nt,)), dma((nt,)), dma((nt,)),
-        sems(nx, 2, True), sems(nz, 2, True), sems(nx, 3, True), sems(nx, 2, True), sems(nz, 2, False), sems(nx, 2, True),
+        vm((nt * rank_q, 1), F32), vm((nt * rank_kv, 1), F32),
+        dma((9,)), dma((nz,)), dma((nz,)), dma((nt,)), dma((nt,)), dma((nt,)), dma((nt,)),
+        sems(nx, 2, True), sems(nz, 2, True), sems(nx, 3, True), sems(nx, 2, True), sems(nz, 2, False), sems(nx, 4, True),
     ]
     here = pl.BlockSpec(memory_space=vm)
     away = pl.BlockSpec(memory_space=pl.ANY)
     small = pl.BlockSpec(memory_space=pltpu.SMEM)
-    return pl.pallas_call(
+    proj, gate = pl.pallas_call(
         functools.partial(kernel, nz, nt),
-        out_shape=jax.ShapeDtypeStruct((rows, width), BF),
+        out_shape=(jax.ShapeDtypeStruct((rows, width), BF), jax.ShapeDtypeStruct((1, width), F32)),
         in_specs=[away, here, away, here, here, here, away, away, away, here, here, away, away, away, small, away],
-        out_specs=here,
+        out_specs=(here, here),
         scratch_shapes=scratch,
         compiler_params=pltpu.CompilerParams(collective_id=0, has_side_effects=True, vmem_limit_bytes=60 * 1024 * 1024),
         name="block",
-    )(latents, conditions, context, w_shift, w_scale, w_gate, w_qdown, w_kvdown, w_rope, q_gain.reshape(1, -1),
-      latent_norm_gain.reshape(1, -1), query_up_weight, key_up_weight, value_up_weight, context_bias.reshape(1, -1), w_out)
+    )(latents, conditions, context, w_shift, w_scale, w_gate, w_qdown.T, w_kvdown.T, w_rope.T, q_gain.reshape(1, -1),
+      latent_norm_gain.reshape(1, -1), query_up_weight.T, key_up_weight, value_up_weight, context_bias.reshape(1, -1), w_out)
+    return (latents.astype(F32) + gate * proj.astype(F32)).astype(BF)
 
 
 def solution(mesh):

time: 203 us -> 176 us (0.87)
  Pallas kernels: 195 us -> 174 us
  local copies, waits for them, and re-layouts: 7.71 us -> 0.01 us
    pallas_call x1, Pallas kernels: 195 us -> 174 us  [on_device(): pl.pallas_call(functools.partial(kernel, nz, nt), out_shape=(jax.ShapeDty...]
    unnamed x11 -> x2, local copies, waits for them, and re-layouts: 7.71 us -> 0.01 us
where the time goes in v2:
time: 176 us
  Pallas kernels  174 us (99%)
    pallas_call x1, Pallas kernels, on_device(): pl.pallas_call(functools.partial(kernel, nz, nt), out_shape=(jax.ShapeDty...  174 us

profile of v2, /device:TPU:65, one launch (start us, length us, event | category | flops | bytes accessed | tf_op | source)
XLA Modules:
  0.0 175.9 jit_solution(3969912998235869548)
XLA Ops:
  0.0 0.0 copy-start
  0.0 174.2 %block.1 = (bf16[24,4096]{1,0:T(8,128)(2,1)}, f32[1,4096]{1,0:T(1,128)}) custom-call(bf16[24,4096]{1,0:T(8,128)(2,1)} %refs_0_.1, f32[2,256]{1,0:T(2,128)} %refs_1_.1, bf16[32,4096]{1,0:T(8,128)(2,1)} %refs_2_.1, bf16[256,256]{1,0:T(8,128)(2,1)} %refs_3_.1, bf16[256,256]{1,0:T(8,128)(2,1)} %refs_4_.1, bf16[256,256]{1,0:T(8,128)(2,1)} %refs_5_.1, ...), custom_call_target="tpu_custom_call" | custom-call | tf_op jit(solution)/shard_map/block/pallas_call | solution.py:510
  174.2 0.0 copy-done
  174.2 1.7 add_convert_fusion
Async XLA Ops:
  0.0 174.2 %copy-start = (bf16[24,4096]{1,0:T(8,128)(2,1)S(1)}, bf16[24,4096]{1,0:T(8,128)(2,1)}, u32[]{:S(2)}) copy-start(bf16[24,4096]{1,0:T(8,128)(2,1)} %refs_0_.1) | copy-start | bytes 589828

commit v3 on v2

--- a/solution.py
+++ b/solution.py
@@ -119,16 +119,16 @@
     (lat_hbm, cond_ref, ctx_hbm, wsh_ref, wsc_ref, wg_ref, wq_hbm, wkv_hbm, wr_hbm, qg_ref, kg_ref,
      uq_hbm, uk_hbm, uv_hbm, bias_ref, wo_hbm, proj_ref, gate_ref,
      lat, ctx, mean_ref, rstd_ref, uk, uv, wo,
-     wcat, uqT, ukvT, zmod, xmod, mod, h, hc, qraw, kvraw, kvcraw, kv, kvc, qb,
-     m_ref, l_ref, acc, att, pbuf, mbuf, q_gain_ref, kv_gain_ref,
-     load_sem, zm_s, zm_r, xm_s, xm_r, a_s, a_r, lat_x, ctx_z, raw_x, rawc_x, kv_z, att_x) = refs
+     wcat, uqT, ukvT, zmod, xmod, mod, h, qraw, kvraw, kv, kvp, kvc, qb,
+     m_ref, l_ref, acc, att, pbuf, mbuf, q_gain_ref, kv_gain_ref, turn_ref,
+     load_sem, zm_s, zm_r, xm_s, xm_r, a_s, a_r, lat_x, raw_x, q_x, kv_z, att_x) = refs
     z, t = lax.axis_index("sp"), lax.axis_index("tp")
     core = lax.rem(t, 2)
     chip = t // 2
     nx = nt // 2
     rows = lat.shape[1]
     tok = rows * nt
-    crows = ctx.shape[1]
+    crows = ctx.shape[0]
     width = lat.shape[2]
     part = width // nt
     rank_q, rank_kv = wq_hbm.shape[0], wkv_hbm.shape[0]
@@ -139,7 +139,7 @@
 
     loads = [
         pltpu.make_async_copy(lat_hbm, lat.at[t], load_sem.at[0]),
-        pltpu.make_async_copy(ctx_hbm, ctx.at[z], load_sem.at[1]),
+        pltpu.make_async_copy(ctx_hbm, ctx, load_sem.at[1]),
         pltpu.make_async_copy(wq_hbm, wcat.at[pl.ds(0, rank_q)], load_sem.at[2]),
         pltpu.make_async_copy(wkv_hbm, wcat.at[pl.ds(rank_q, rank_kv)], load_sem.at[3]),
         pltpu.make_async_copy(wr_hbm, wcat.at[pl.ds(rank_q + rank_kv, ROTARY)], load_sem.at[4]),
@@ -185,17 +185,7 @@
                       [lambda p, c: lat.at[2 * p + c, :, pl.ds(0, half)], lambda p, c: lat.at[2 * p + c, :, pl.ds(half, half)]],
                       lat_x, partner, core)
     lat_ring.start()
-    loads[1].wait()
-    quarter = half // 2
-    at_half = lambda c, q: pl.ds(pl.multiple_of(c * half + q * quarter, 128), quarter)
-    ctx_ring = Gather(nz, z, along_z,
-                      [lambda p, c: ctx.at[p, :, at_half(c, 0)], lambda p, c: ctx.at[p, :, at_half(c, 1)]],
-                      ctx_z, partner, core)
-    for ch in range(2):
-        for d in range(2):
-            ctx_ring.ring_copy(d, 0, ch).start()
-
-    for load in loads[2:]:
+    for load in loads[1:]:
         load.wait()
     ukvT[0:2 * PLAIN, :] = uk[...].astype(F32).T.astype(BF)
     ukvT[2 * PLAIN:2 * PLAIN + VROWS, :] = uv[...].astype(F32).T.astype(BF)
@@ -207,21 +197,6 @@
     col_angle = (pos & (GRID_W - 1)).astype(F32) * freq
     turn = (jnp.cos(row_angle), jnp.sin(row_angle), jnp.cos(col_angle), jnp.sin(col_angle))
 
-    def ctx_step(s):
-        for ch in range(2):
-            for d in range(2):
-                if ctx_ring.active(d, s, ch):
-                    ctx_ring.ring_arrival(d, s, ch).wait_recv()
-                    if ctx_ring.active(d, s + 1, ch):
-                        ctx_ring.ring_copy(d, s, ch).start()
-                    ctx_ring.pair_copy(d, s, ch, core).start()
-
-    steps_z = list(range(1, ctx_ring.reach + 1))
-
-    def ctx_next(least=0):
-        if len(steps_z) > least:
-            ctx_step(steps_z.pop(0))
-
     def chip_rows(p):
         return jnp.concatenate([lat[2 * p].astype(F32), lat[2 * p + 1].astype(F32)], axis=0)
 
@@ -232,7 +207,6 @@
         rstd_ref[p] = lax.rsqrt(jnp.mean(center * center, axis=-1, keepdims=True) + EPSILON)
 
     lat_ring.step(1)
-    ctx_next()
     for k in reversed(order):
         zm(k, True).wait_recv()
     total = zmod[0]
@@ -250,7 +224,6 @@
             note_statistics(lax.rem(chip + jnp.where(i == 0, nx - (s - 2), s - 2), nx))
 
         lat_ring.step(s)
-        ctx_next()
     lat_ring.pair_step(far - 1)
 
     @pl.loop(0, 2 if far > 1 else 1)
@@ -264,52 +237,69 @@
     for j in range(nt):
         mod[:, j * part:(j + 1) * part] = xmod[j]
 
-    for piece in range(2):
-        @pl.loop(piece * nx // 2, (piece + 1) * nx // 2)
-        def _(p):
-            at = pl.ds(pl.multiple_of(p * 2 * rows, 2 * rows), 2 * rows)
-            normed = (chip_rows(p) - mean_ref[p]) * rstd_ref[p]
-            h[at, :] = (normed * (1.0 + mod[2:3, :]) + mod[0:1, :]).astype(BF)
-        ctx_next()
-
-    raw = lax.dot_general(h[...], wcat[...], (((1,), (1,)), ((), ())), preferred_element_type=F32).T
+    @pl.loop(0, nx)
+    def _(p):
+        at = pl.ds(pl.multiple_of(p * 2 * rows, 2 * rows), 2 * rows)
+        normed = (chip_rows(p) - mean_ref[p]) * rstd_ref[p]
+        h[at, :] = (normed * (1.0 + mod[2:3, :]) + mod[0:1, :]).astype(BF)
+
+    h[tok:, :] = modulated(ctx[...], mod[1:2, :], mod[3:4, :])
+    product = lax.dot_general(h[...], wcat[...], (((1,), (1,)), ((), ())), preferred_element_type=F32)
+    raw = product[0:tok].T
+    rawc = jnp.concatenate([product[tok:], jnp.zeros((128 - crows, product.shape[1]), F32)], axis=0).T
     q_at = lambda p, c, i: pl.ds(pl.multiple_of((2 * p + c) * rank_q + i * (rank_q // 2), rank_q // 2), rank_q // 2)
     kv_at = lambda p, c: pl.ds(pl.multiple_of((2 * p + c) * rank_kv, rank_kv), rank_kv)
-    qraw[pl.ds(pl.multiple_of(t * rank_q, rank_q), rank_q), :] = raw[0:rank_q].astype(BF)
-    kvraw[kv_at(chip, core), :] = raw[rank_q:rank_q + rank_kv].astype(BF)
+    kvraw[kv_at(chip, core), 0:tok] = raw[rank_q:rank_q + rank_kv].astype(BF)
+    kvraw[kv_at(chip, core), tok:] = rawc[rank_q:rank_q + rank_kv].astype(BF)
+    lane_half = kvraw.shape[1] // 2
     raw_ring = Gather(nx, chip, along_x,
-                      [lambda p, c: kvraw.at[kv_at(p, c), :], lambda p, c: qraw.at[q_at(p, c, 0), :], lambda p, c: qraw.at[q_at(p, c, 1), :]],
+                      [lambda p, c: kvraw.at[kv_at(p, c), pl.ds(0, lane_half)], lambda p, c: kvraw.at[kv_at(p, c), pl.ds(lane_half, lane_half)]],
                       raw_x, partner, core)
     raw_ring.start()
+    qraw[pl.ds(pl.multiple_of(t * rank_q, rank_q), rank_q), :] = raw[0:rank_q].astype(BF)
+    q_ring = Gather(nx, chip, along_x,
+                    [lambda p, c: qraw.at[q_at(p, c, 0), :], lambda p, c: qraw.at[q_at(p, c, 1), :]],
+                    q_x, partner, core)
+    q_ring.start()
     kv[z, 2 * PLAIN:KROWS, :] = axial_turn(raw[rank_q + rank_kv:], *turn).astype(BF)
+    for i in range(4):
+        turn_ref[i] = turn[i]
 
     for s in range(1, raw_ring.reach + 1):
         raw_ring.step(s)
-        if s == 2:
-            ctx_next(1)
     for s in range(0, raw_ring.reach + 1):
         raw_ring.pair_step(s)
 
     ckv = rms_columns(kvraw[...], kv_gain_ref[...])
     own = jnp.dot(ukvT[...], ckv, preferred_element_type=F32).astype(BF)
-    kv[z, 0:2 * PLAIN, :] = own[0:2 * PLAIN]
-    kv[z, KROWS:KROWS + VROWS, :] = own[2 * PLAIN:]
+    kv[z, 0:2 * PLAIN, :] = own[0:2 * PLAIN, 0:tok]
+    kv[z, KROWS:KROWS + VROWS, :] = own[2 * PLAIN:, 0:tok]
+    loose = jnp.concatenate([own[0:2 * PLAIN, tok:].astype(F32), rawc[rank_q + rank_kv:].astype(BF).astype(F32), own[2 * PLAIN:, tok:].astype(F32)], axis=0)
+    group = (KROWS + VROWS) // 4
+    packed = loose[0:group]
+    for g in range(1, 4):
+        packed = packed + pltpu.roll(loose[g * group:(g + 1) * group], g * crows, 1)
+    kvp[z] = jnp.concatenate([packed, jnp.zeros((kvp.shape[1] - group, 128), F32)], axis=0).astype(BF)
     kv_half = (KROWS + VROWS) // 2
-    kv_ring = Gather(nz, z, along_z, [lambda p, c: kv.at[p, pl.ds(0, kv_half)], lambda p, c: kv.at[p, pl.ds(kv_half, kv_half)]], kv_z)
+    kv_chunks = [lambda p, c: kv.at[p, pl.ds(0, kv_half)], lambda p, c: kv.at[p, pl.ds(kv_half, kv_half)], lambda p, c: kvp.at[p]]
+    kv_ring = Gather(nz, z, along_z, kv_chunks, kv_z)
+    kv_ring.cut = 1
     kv_ring.start()
-    while len(steps_z) > 1:
-        ctx_next()
-
-    cq = rms_columns(qraw[...], q_gain_ref[...])
-    q = jnp.dot(uqT[...], cq, preferred_element_type=F32)
-    per = PLAIN + ROTARY
-    for head in range(2):
-        mine = q[head * per:(head + 1) * per]
-        plain = mine[0:PLAIN].astype(BF)
-        blank = jnp.zeros_like(plain)
-        qb[head, head * PLAIN:(head + 1) * PLAIN, :] = plain
-        qb[head, (1 - head) * PLAIN:(2 - head) * PLAIN, :] = blank
-        qb[head, 2 * PLAIN:KROWS, :] = axial_turn(mine[PLAIN:], *turn).astype(BF)
+
+    def query_up():
+        for s in range(0, q_ring.reach + 1):
+            q_ring.pair_step(s)
+        cq = rms_columns(qraw[...], q_gain_ref[...])
+        q = jnp.dot(uqT[...], cq, preferred_element_type=F32)
+        per = PLAIN + ROTARY
+        for head in range(2):
+            mine = q[head * per:(head + 1) * per]
+            plain = mine[0:PLAIN].astype(BF)
+            blank = jnp.zeros_like(plain)
+            qb[head, head * PLAIN:(head + 1) * PLAIN, :] = plain
+            qb[head, (1 - head) * PLAIN:(2 - head) * PLAIN, :] = blank
+            qb[head, 2 * PLAIN:KROWS, :] = axial_turn(mine[PLAIN:], *[turn_ref[i] for i in range(4)]).astype(BF)
+
     m_ref[...] = jnp.full_like(m_ref, NEGATIVE)
     l_ref[...] = jnp.zeros_like(l_ref)
     acc[...] = jnp.zeros_like(acc)
@@ -328,100 +318,91 @@
             l_ref[head] = l_ref[head] * alpha + jnp.sum(e, axis=0, keepdims=True)
             acc[head] = acc[head] * alpha + jnp.dot(valuesT[head * VALUE:(head + 1) * VALUE], e.astype(BF), preferred_element_type=F32)
 
-    attend(kv[z, 0:KROWS, :], kv[z, KROWS:KROWS + VROWS, :], False)
-    while steps_z:
-        ctx_next()
-    for s in range(1, ctx_ring.reach + 1):
-        ctx_ring.pair_step(s)
-    chalf = kvcraw.shape[1] // 2
-    rawc_ring = Gather(nx, chip, along_x,
-                       [lambda p, c: kvcraw.at[kv_at(p, c), pl.ds(0, chalf)], lambda p, c: kvcraw.at[kv_at(p, c), pl.ds(chalf, chalf)]],
-                       rawc_x, partner, core)
     reach = kv_ring.reach
 
     def ring_source(d, s):
         return lax.rem(z + jnp.where(d == 0, nz - s, s), nz)
 
+    def nth_source(n):
+        return ring_source(1 - lax.rem(n, 2), (n + 1) // 2)
+
     def hop(d, s, ch, into):
-        piece = kv.at[ring_source(d, s), pl.ds(ch * kv_half, kv_half)]
+        piece = kv_chunks[ch](ring_source(d, s), 0)
         return pltpu.make_async_remote_copy(piece, piece, kv_z[1].at[d, s, ch], kv_z[0].at[d, into, ch],
                                             device_id=along_z(1 if d == 0 else nz - 1), device_id_type=MESH)
 
     def pass_on(s, ch):
         for d in range(2):
             hop(d, s, ch, s).wait_recv()
-        for d in range(2):
-            if d == ch:
+            if d == min(ch, 1):
                 hop(d, s, ch, s + 1).start()
             else:
                 @pl.when(s + 1 < reach)
                 def _():
                     hop(d, s, ch, s + 1).start()
 
-    def attend_block(d, s):
-        b = ring_source(d, s)
+    def attend_block(n):
+        b = nth_source(n)
         attend(kv[b, 0:KROWS, :], kv[b, KROWS:KROWS + VROWS, :], False)
 
-    def context_quarter(quarter):
-        @pl.loop(quarter * nz // 4, (quarter + 1) * nz // 4)
-        def _(i):
-            at = pl.ds(pl.multiple_of(i * crows, crows), crows)
-            hc[at, :] = modulated(ctx[i], mod[1:2, :], mod[3:4, :])
-
-    def context_down():
-        rawc = lax.dot_general(hc[...], wcat[...], (((1,), (1,)), ((), ())), preferred_element_type=F32).T
-        kvcraw[kv_at(chip, core), :] = rawc[rank_q:rank_q + rank_kv].astype(BF)
-        kvc[2 * PLAIN:KROWS, :] = rawc[rank_q + rank_kv:].astype(BF)
-        rawc_ring.start()
-
-    def context_up():
-        for s in range(0, rawc_ring.reach + 1):
-            rawc_ring.pair_step(s)
-        ckvc = rms_columns(kvcraw[...], kv_gain_ref[...])
-        ownc = jnp.dot(ukvT[...], ckvc, preferred_element_type=F32).astype(BF)
-        kvc[0:2 * PLAIN, :] = ownc[0:2 * PLAIN]
-        kvc[KROWS:KROWS + VROWS, :] = ownc[2 * PLAIN:]
-
-    jobs = [functools.partial(context_quarter, i) for i in range(4)] + [context_down]
-    jobs += [functools.partial(rawc_ring.step, s) for s in range(1, rawc_ring.reach + 1)] + [context_up]
+    def unpack(tile):
+        lanes = lax.broadcasted_iota(jnp.int32, (group, 128), 1) // crows
+        parts = [None] * 4
+        for j in range(4):
+            held = kvp[nth_source(4 * tile + j)][0:group].astype(F32)
+            for g in range(4):
+                moved = jnp.where(lanes == g, held, 0.0)
+                if g != j:
+                    moved = pltpu.roll(moved, ((j - g) % 4) * crows, 1)
+                parts[g] = moved if parts[g] is None else parts[g] + moved
+        kvc[:, tile * 128:(tile + 1) * 128] = jnp.concatenate(parts, axis=0).astype(BF)
+
     slots = 2 * (reach - 1)
-    place = {}
-    for i, job in enumerate(jobs):
-        spare = i if i < 5 else 5 + 2 * (i - 5) + 1
-        place.setdefault(min(spare, slots - 1), []).append(job)
-
-    def do_jobs(slot, now):
-        for at, work in place.items():
-            if at % 2 == slot:
-                @pl.when(now == at // 2 + 1)
-                def _():
-                    for job in work:
-                        job()
-
-    def kv_step(s, carry):
-        pass_on(s, 0)
-
-        @pl.when(s > 1)
+    first = min(q_ring.reach, slots)
+
+    def done_after(i):
+        return jnp.clip(2 * (i - first + 1), 0, i + 1)
+
+    def kv_slot(i, carry):
+        s = i // 2 + 1
+
+        @pl.when(lax.rem(i, 2) == 0)
         def _():
-            attend_block(0, s - 1)
-        do_jobs(0, s)
-        pass_on(s, 1)
-
-        @pl.when(s > 1)
+            pass_on(s, 0)
+
+        @pl.when(lax.rem(i, 2) == 1)
         def _():
-            attend_block(1, s - 1)
-        do_jobs(1, s)
+            pass_on(s, 1)
+            pass_on(s, 2)
+
+        for step in range(1, q_ring.reach + 1):
+            @pl.when(i == min(step, first) - 1)
+            def _():
+                q_ring.step(step)
+                if step == q_ring.reach:
+                    query_up()
+
+        @pl.loop(jnp.where(i >= first, done_after(i - 1), 0), jnp.where(i >= first, done_after(i), 0))
+        def _(n):
+            attend_block(n)
         return carry
 
-    lax.fori_loop(1, reach, kv_step, 0)
-
-    @pl.loop(0, 2)
-    def _(d):
-        attend_block(d, reach - 1)
-    attend(kvc[0:KROWS, :], kvc[KROWS:KROWS + VROWS, :], True)
+    lax.fori_loop(0, slots, kv_slot, 0)
+
+    @pl.loop(done_after(slots - 1), 2 * reach - 1)
+    def _(n):
+        attend_block(n)
+    tiles = nz // 4
+    for tile in range(tiles - 1):
+        unpack(tile)
+    if tiles > 1:
+        attend(kvc[0:KROWS, 0:128 * (tiles - 1)], kvc[KROWS:KROWS + VROWS, 0:128 * (tiles - 1)], True)
     kv_ring.ring_arrival(0, reach, 0).wait_recv()
     kv_ring.ring_arrival(1, reach, 1).wait_recv()
-    attend_block(0, reach)
+    kv_ring.ring_arrival(1, reach, 2).wait_recv()
+    attend_block(2 * reach - 1)
+    unpack(tiles - 1)
+    attend(kvc[0:KROWS, 128 * (tiles - 1):], kvc[KROWS:KROWS + VROWS, 128 * (tiles - 1):], True)
 
     outT = jnp.concatenate([acc[0] / l_ref[0], acc[1] / l_ref[1]], axis=0)
     mine_at = lambda p, c: pl.ds(pl.multiple_of((2 * p + c) * VROWS, VROWS), VROWS)
@@ -461,15 +442,8 @@
         xm(k, False).wait_send()
         am(k, False).wait_send()
     lat_ring.finish()
-    for s in range(ctx_ring.reach + 1):
-        for ch in range(2):
-            for d in range(2):
-                if ctx_ring.active(d, s + 1, ch):
-                    ctx_ring.ring_copy(d, s, ch).wait_send()
-                if s > 0 and ctx_ring.active(d, s, ch):
-                    ctx_ring.pair_copy(d, s, ch, core).wait_send()
     raw_ring.finish()
-    rawc_ring.finish()
+    q_ring.finish()
     kv_ring.finish()
     att_ring.finish()
 
@@ -491,18 +465,18 @@
     vm = pltpu.VMEM
     dma = pltpu.SemaphoreType.DMA
     scratch = [
-        vm((nt, rows, width), BF), vm((nz, crows, width), BF), vm((nx, 2 * rows, 1), F32), vm((nx, 2 * rows, 1), F32),
+        vm((nt, rows, width), BF), vm((crows, width), BF), vm((nx, 2 * rows, 1), F32), vm((nx, 2 * rows, 1), F32),
         vm(key_up_weight.shape, BF), vm(value_up_weight.shape, BF), vm(w_out.shape, BF),
         vm((rank_q + rank_kv + ROTARY, width), BF), vm(query_up_weight.shape[::-1], BF), vm((2 * PLAIN + VROWS, nt * rank_kv), BF),
         vm((nz, 8, part), F32), vm((nt, 8, part), F32), vm((8, width), F32),
-        vm((tok, width), BF), vm((nz * crows, width), BF),
-        vm((nt * rank_q, tok), BF), vm((nt * rank_kv, tok), BF), vm((nt * rank_kv, nz * crows), BF),
-        vm((nz, KROWS + VROWS, tok), BF), vm((KROWS + VROWS, nz * crows), BF), vm((2, KROWS, tok), BF),
+        vm((tok + crows, width), BF),
+        vm((nt * rank_q, tok), BF), vm((nt * rank_kv, tok + 128), BF),
+        vm((nz, KROWS + VROWS, tok), BF), vm((nz, 80, 128), BF), vm((KROWS + VROWS, nz * crows), BF), vm((2, KROWS, tok), BF),
         vm((2, 1, tok), F32), vm((2, 1, tok), F32), vm((2, VALUE, tok), F32),
         vm((tok, nt * VROWS), BF), vm((nt, rows, part), BF), vm((nt, rows, part), BF),
-        vm((nt * rank_q, 1), F32), vm((nt * rank_kv, 1), F32),
+        vm((nt * rank_q, 1), F32), vm((nt * rank_kv, 1), F32), vm((4, 8, tok), F32),
         dma((9,)), dma((nz,)), dma((nz,)), dma((nt,)), dma((nt,)), dma((nt,)), dma((nt,)),
-        sems(nx, 2, True), sems(nz, 2, True), sems(nx, 3, True), sems(nx, 2, True), sems(nz, 2, False), sems(nx, 4, True),
+        sems(nx, 2, True), sems(nx, 2, True), sems(nx, 2, True), sems(nz, 3, False), sems(nx, 4, True),
     ]
     here = pl.BlockSpec(memory_space=vm)
     away = pl.BlockSpec(memory_space=pl.ANY)

time: 176 us -> 167 us (0.949)
  Pallas kernels: 174 us -> 166 us
    pallas_call x1, Pallas kernels: 174 us -> 166 us  [on_device(): pl.pallas_call(functools.partial(kernel, nz, nt), out_shape=(jax.ShapeDty...]
where the time goes in v3:
time: 167 us
  Pallas kernels  166 us (99%)
  other arithmetic  1.67 us (1%)
    pallas_call x1, Pallas kernels, on_device(): pl.pallas_call(functools.partial(kernel, nz, nt), out_shape=(jax.ShapeDty...  166 us

profile of v3, /device:TPU:65, one launch (start us, length us, event | category | flops | bytes accessed | tf_op | source)
XLA Modules:
  0.0 167.3 jit_solution(7351893389614807033)
XLA Ops:
  0.0 0.0 copy-start
  0.0 165.6 %block.1 = (bf16[24,4096]{1,0:T(8,128)(2,1)}, f32[1,4096]{1,0:T(1,128)}) custom-call(bf16[24,4096]{1,0:T(8,128)(2,1)} %refs_0_.1, f32[2,256]{1,0:T(2,128)} %refs_1_.1, bf16[32,4096]{1,0:T(8,128)(2,1)} %refs_2_.1, bf16[256,256]{1,0:T(8,128)(2,1)} %refs_3_.1, bf16[256,256]{1,0:T(8,128)(2,1)} %refs_4_.1, bf16[256,256]{1,0:T(8,128)(2,1)} %refs_5_.1, ...), custom_call_target="tpu_custom_call" | custom-call | tf_op jit(solution)/shard_map/block/pallas_call | solution.py:484
  165.6 0.0 copy-done
  165.6 1.7 add_convert_fusion
Async XLA Ops:
  0.0 165.6 %copy-start = (bf16[24,4096]{1,0:T(8,128)(2,1)S(1)}, bf16[24,4096]{1,0:T(8,128)(2,1)}, u32[]{:S(2)}) copy-start(bf16[24,4096]{1,0:T(8,128)(2,1)} %refs_0_.1) | copy-start | bytes 589828

commit v4 on v3

--- a/solution.py
+++ b/solution.py
@@ -121,7 +121,7 @@
      lat, ctx, mean_ref, rstd_ref, uk, uv, wo,
      wcat, uqT, ukvT, zmod, xmod, mod, h, qraw, kvraw, kv, kvp, kvc, qb,
      m_ref, l_ref, acc, att, pbuf, mbuf, q_gain_ref, kv_gain_ref, turn_ref,
-     load_sem, zm_s, zm_r, xm_s, xm_r, a_s, a_r, lat_x, raw_x, q_x, kv_z, att_x) = refs
+     load_sem, zm_s, zm_r, xm_s, xm_r, a_s, a_r, lat_x, raw_s, raw_r, rawp_s, rawp_r, q_x, kv_z, kr_s, kr_r, att_x) = refs
     z, t = lax.axis_index("sp"), lax.axis_index("tp")
     core = lax.rem(t, 2)
     chip = t // 2
@@ -135,7 +135,7 @@
     along_z = lambda k: {"sp": lax.rem(z + k, nz)}
     along_x = lambda k: {"tp": lax.rem(t + 2 * k, nt)}
     partner = {"tp": t + 1 - 2 * core}
-    half = width // 2
+    fourth_of_width = width // 4
 
     loads = [
         pltpu.make_async_copy(lat_hbm, lat.at[t], load_sem.at[0]),
@@ -182,7 +182,7 @@
         zm(k, False).start()
     loads[0].wait()
     lat_ring = Gather(nx, chip, along_x,
-                      [lambda p, c: lat.at[2 * p + c, :, pl.ds(0, half)], lambda p, c: lat.at[2 * p + c, :, pl.ds(half, half)]],
+                      [lambda p, c, i=i: lat.at[2 * p + c, :, pl.ds(i * fourth_of_width, fourth_of_width)] for i in range(4)],
                       lat_x, partner, core)
     lat_ring.start()
     for load in loads[1:]:
@@ -252,38 +252,65 @@
     kvraw[kv_at(chip, core), 0:tok] = raw[rank_q:rank_q + rank_kv].astype(BF)
     kvraw[kv_at(chip, core), tok:] = rawc[rank_q:rank_q + rank_kv].astype(BF)
     lane_half = kvraw.shape[1] // 2
-    raw_ring = Gather(nx, chip, along_x,
-                      [lambda p, c: kvraw.at[kv_at(p, c), pl.ds(0, lane_half)], lambda p, c: kvraw.at[kv_at(p, c), pl.ds(lane_half, lane_half)]],
-                      raw_x, partner, core)
-    raw_ring.start()
+    opposite = nx // 2
+
+    def raw_piece(k, side, c):
+        piece = kvraw.at[kv_at(lax.rem(chip + nx - k, nx), c)]
+        return piece if side is None else kvraw.at[kv_at(lax.rem(chip + nx - k, nx), c), pl.ds(side * lane_half, lane_half)]
+
+    def raw_copy(k, incoming):
+        piece = raw_piece(k if incoming else 0, None, core)
+        return pltpu.make_async_remote_copy(piece, piece, raw_s.at[k], raw_r.at[k], device_id=along_x(k), device_id_type=MESH)
+
+    def raw_last(side, incoming):
+        near = 1 if side == 0 else nx - 1
+        piece = raw_piece(opposite if incoming else near, side, core)
+        at = opposite if side == 0 else nx
+        return pltpu.make_async_remote_copy(piece, piece, raw_s.at[at], raw_r.at[at],
+                                            device_id=along_x(opposite - 1 if side == 0 else nx - opposite + 1), device_id_type=MESH)
+
+    def raw_pair(k, incoming):
+        piece = raw_piece(k, None, 1 - core if incoming else core)
+        return pltpu.make_async_remote_copy(piece, piece, rawp_s.at[k], rawp_r.at[k], device_id=partner, device_id_type=MESH)
+
+    by_distance = [k for m in range(1, opposite) for k in (m, nx - m)]
+    for k in by_distance:
+        raw_copy(k, False).start()
+    raw_pair(0, False).start()
     qraw[pl.ds(pl.multiple_of(t * rank_q, rank_q), rank_q), :] = raw[0:rank_q].astype(BF)
     q_ring = Gather(nx, chip, along_x,
                     [lambda p, c: qraw.at[q_at(p, c, 0), :], lambda p, c: qraw.at[q_at(p, c, 1), :]],
                     q_x, partner, core)
     q_ring.start()
-    kv[z, 2 * PLAIN:KROWS, :] = axial_turn(raw[rank_q + rank_kv:], *turn).astype(BF)
+    own_last = lambda a: jnp.where(core == 0, jnp.concatenate([a[ROTARY // 2:], a[:ROTARY // 2]], axis=0), a)
+    kv[z, 2 * PLAIN:KROWS, :] = own_last(axial_turn(raw[rank_q + rank_kv:], *turn)).astype(BF)
     for i in range(4):
         turn_ref[i] = turn[i]
-
-    for s in range(1, raw_ring.reach + 1):
-        raw_ring.step(s)
-    for s in range(0, raw_ring.reach + 1):
-        raw_ring.pair_step(s)
+    for k in by_distance:
+        raw_copy(k, True).wait_recv()
+        if k in (1, nx - 1):
+            raw_last(0 if k == 1 else 1, False).start()
+        raw_pair(k, False).start()
+    for side in range(2):
+        raw_last(side, True).wait_recv()
+    raw_pair(opposite, False).start()
+    for k in range(nx):
+        raw_pair(k, True).wait_recv()
 
     ckv = rms_columns(kvraw[...], kv_gain_ref[...])
     own = jnp.dot(ukvT[...], ckv, preferred_element_type=F32).astype(BF)
     kv[z, 0:2 * PLAIN, :] = own[0:2 * PLAIN, 0:tok]
     kv[z, KROWS:KROWS + VROWS, :] = own[2 * PLAIN:, 0:tok]
-    loose = jnp.concatenate([own[0:2 * PLAIN, tok:].astype(F32), rawc[rank_q + rank_kv:].astype(BF).astype(F32), own[2 * PLAIN:, tok:].astype(F32)], axis=0)
+    loose = jnp.concatenate([own[0:2 * PLAIN, tok:].astype(F32), own_last(rawc[rank_q + rank_kv:]).astype(BF).astype(F32), own[2 * PLAIN:, tok:].astype(F32)], axis=0)
     group = (KROWS + VROWS) // 4
     packed = loose[0:group]
     for g in range(1, 4):
         packed = packed + pltpu.roll(loose[g * group:(g + 1) * group], g * crows, 1)
     kvp[z] = jnp.concatenate([packed, jnp.zeros((kvp.shape[1] - group, 128), F32)], axis=0).astype(BF)
-    kv_half = (KROWS + VROWS) // 2
-    kv_chunks = [lambda p, c: kv.at[p, pl.ds(0, kv_half)], lambda p, c: kv.at[p, pl.ds(kv_half, kv_half)], lambda p, c: kvp.at[p]]
+    kr_half = ROTARY // 2
+    kv_chunks = [lambda p, c: kv.at[p, pl.ds(0, 2 * PLAIN)], lambda p, c: kvp.at[p],
+                 lambda p, c: kv.at[p, pl.ds(2 * PLAIN + kr_half, kr_half + VROWS)]]
     kv_ring = Gather(nz, z, along_z, kv_chunks, kv_z)
-    kv_ring.cut = 1
     kv_ring.start()
 
     def query_up():
@@ -298,7 +325,7 @@
             blank = jnp.zeros_like(plain)
             qb[head, head * PLAIN:(head + 1) * PLAIN, :] = plain
             qb[head, (1 - head) * PLAIN:(2 - head) * PLAIN, :] = blank
-            qb[head, 2 * PLAIN:KROWS, :] = axial_turn(mine[PLAIN:], *[turn_ref[i] for i in range(4)]).astype(BF)
+            qb[head, 2 * PLAIN:KROWS, :] = own_last(axial_turn(mine[PLAIN:], *[turn_ref[i] for i in range(4)])).astype(BF)
 
     m_ref[...] = jnp.full_like(m_ref, NEGATIVE)
     l_ref[...] = jnp.zeros_like(l_ref)
@@ -331,15 +358,23 @@
         return pltpu.make_async_remote_copy(piece, piece, kv_z[1].at[d, s, ch], kv_z[0].at[d, into, ch],
                                             device_id=along_z(1 if d == 0 else nz - 1), device_id_type=MESH)
 
+    def kr_swap(d, s, incoming):
+        b = ring_source(d, s)
+        mine, theirs = kv.at[b, pl.ds(2 * PLAIN + kr_half, kr_half)], kv.at[b, pl.ds(2 * PLAIN, kr_half)]
+        return pltpu.make_async_remote_copy(theirs if incoming else mine, theirs, kr_s.at[d, s], kr_r.at[d, s],
+                                            device_id=partner, device_id_type=MESH)
+
     def pass_on(s, ch):
         for d in range(2):
             hop(d, s, ch, s).wait_recv()
-            if d == min(ch, 1):
+            if d == ch // 2:
                 hop(d, s, ch, s + 1).start()
             else:
                 @pl.when(s + 1 < reach)
                 def _():
                     hop(d, s, ch, s + 1).start()
+            if ch == 2:
+                kr_swap(d, s, False).start()
 
     def attend_block(n):
         b = nth_source(n)
@@ -361,7 +396,7 @@
     first = min(q_ring.reach, slots)
 
     def done_after(i):
-        return jnp.clip(2 * (i - first + 1), 0, i + 1)
+        return jnp.clip(2 * (i - first + 1), 0, i)
 
     def kv_slot(i, carry):
         s = i // 2 + 1
@@ -369,10 +404,15 @@
         @pl.when(lax.rem(i, 2) == 0)
         def _():
             pass_on(s, 0)
+            pass_on(s, 1)
+
+            @pl.when(s > 1)
+            def _():
+                for d in range(2):
+                    kr_swap(d, s - 1, True).wait_recv()
 
         @pl.when(lax.rem(i, 2) == 1)
         def _():
-            pass_on(s, 1)
             pass_on(s, 2)
 
         for step in range(1, q_ring.reach + 1):
@@ -388,6 +428,8 @@
         return carry
 
     lax.fori_loop(0, slots, kv_slot, 0)
+    for d in range(2):
+        kr_swap(d, reach - 1, True).wait_recv()
 
     @pl.loop(done_after(slots - 1), 2 * reach - 1)
     def _(n):
@@ -398,10 +440,12 @@
     if tiles > 1:
         attend(kvc[0:KROWS, 0:128 * (tiles - 1)], kvc[KROWS:KROWS + VROWS, 0:128 * (tiles - 1)], True)
     kv_ring.ring_arrival(0, reach, 0).wait_recv()
-    kv_ring.ring_arrival(1, reach, 1).wait_recv()
+    kv_ring.ring_arrival(0, reach, 1).wait_recv()
     kv_ring.ring_arrival(1, reach, 2).wait_recv()
+    kr_swap(0, reach, False).start()
+    unpack(tiles - 1)
+    kr_swap(0, reach, True).wait_recv()
     attend_block(2 * reach - 1)
-    unpack(tiles - 1)
     attend(kvc[0:KROWS, 128 * (tiles - 1):], kvc[KROWS:KROWS + VROWS, 128 * (tiles - 1):], True)
 
     outT = jnp.concatenate([acc[0] / l_ref[0], acc[1] / l_ref[1]], axis=0)
@@ -442,7 +486,15 @@
         xm(k, False).wait_send()
         am(k, False).wait_send()
     lat_ring.finish()
-    raw_ring.finish()
+    for k in by_distance:
+        raw_copy(k, False).wait_send()
+    for side in range(2):
+        raw_last(side, False).wait_send()
+    for k in range(nx):
+        raw_pair(k, False).wait_send()
+    for s in range(1, reach + 1):
+        for d in range(2 if s < reach else 1):
+            kr_swap(d, s, False).wait_send()
     q_ring.finish()
     kv_ring.finish()
     att_ring.finish()
@@ -476,7 +528,8 @@
         vm((tok, nt * VROWS), BF), vm((nt, rows, part), BF), vm((nt, rows, part), BF),
         vm((nt * rank_q, 1), F32), vm((nt * rank_kv, 1), F32), vm((4, 8, tok), F32),
         dma((9,)), dma((nz,)), dma((nz,)), dma((nt,)), dma((nt,)), dma((nt,)), dma((nt,)),
-        sems(nx, 2, True), sems(nx, 2, True), sems(nx, 2, True), sems(nz, 3, False), sems(nx, 4, True),
+        sems(nx, 4, True), dma((nx + 1,)), dma((nx + 1,)), dma((nx,)), dma((nx,)), sems(nx, 2, True), sems(nz, 3, False),
+        dma((2, nz // 2 + 1)), dma((2, nz // 2 + 1)), sems(nx, 4, True),
     ]
     here = pl.BlockSpec(memory_space=vm)
     away = pl.BlockSpec(memory_space=pl.ANY)

time: 167 us -> 166 us (level)
  Pallas kernels: 166 us -> 164 us
    pallas_call x1, Pallas kernels: 166 us -> 164 us  [on_device(): pl.pallas_call(functools.partial(kernel, nz, nt), out_shape=(jax.ShapeDty...]
where the time goes in v4:
time: 166 us
  Pallas kernels  164 us (99%)
  other arithmetic  1.67 us (1%)
    pallas_call x1, Pallas kernels, on_device(): pl.pallas_call(functools.partial(kernel, nz, nt), out_shape=(jax.ShapeDty...  164 us

profile of v4, /device:TPU:65, one launch (start us, length us, event | category | flops | bytes accessed | tf_op | source)
XLA Modules:
  0.0 165.6 jit_solution(4163536489141550494)
XLA Ops:
  0.0 0.0 copy-start
  0.0 163.9 %block.1 = (bf16[24,4096]{1,0:T(8,128)(2,1)}, f32[1,4096]{1,0:T(1,128)}) custom-call(bf16[24,4096]{1,0:T(8,128)(2,1)} %refs_0_.1, f32[2,256]{1,0:T(2,128)} %refs_1_.1, bf16[32,4096]{1,0:T(8,128)(2,1)} %refs_2_.1, bf16[256,256]{1,0:T(8,128)(2,1)} %refs_3_.1, bf16[256,256]{1,0:T(8,128)(2,1)} %refs_4_.1, bf16[256,256]{1,0:T(8,128)(2,1)} %refs_5_.1, ...), custom_call_target="tpu_custom_call" | custom-call | tf_op jit(solution)/shard_map/block/pallas_call | solution.py:537
  163.9 0.0 copy-done
  163.9 1.7 %add_convert_fusion = bf16[24,4096]{1,0:T(8,128)(2,1)} fusion(bf16[24,4096]{1,0:T(8,128)(2,1)} %get-tuple-element.8, bf16[24,4096]{1,0:T(8,128)(2,1)S(1)} %copy-done, f32[4096]{0:T(1024)} %bitcast.12), kind=kLoop, calls=%fused_computation | loop fusion | flops 491520 | bytes 606208 | tf_op jit(solution)/shard_map/convert_element_type | solution.py:547
Async XLA Ops:
  0.0 163.9 %copy-start = (bf16[24,4096]{1,0:T(8,128)(2,1)S(1)}, bf16[24,4096]{1,0:T(8,128)(2,1)}, u32[]{:S(2)}) copy-start(bf16[24,4096]{1,0:T(8,128)(2,1)} %refs_0_.1) | copy-start | bytes 589828

commit v5 on v4

--- a/solution.py
+++ b/solution.py
@@ -207,14 +207,6 @@
         rstd_ref[p] = lax.rsqrt(jnp.mean(center * center, axis=-1, keepdims=True) + EPSILON)
 
     lat_ring.step(1)
-    for k in reversed(order):
-        zm(k, True).wait_recv()
-    total = zmod[0]
-    for k in range(1, nz):
-        total = total + zmod[k]
-    xmod[t] = total
-    for k in range(1, nt):
-        xm(k, False).start()
     far = lat_ring.reach
     for s in range(2, far + 1):
         lat_ring.pair_step(s - 2)
@@ -224,6 +216,15 @@
             note_statistics(lax.rem(chip + jnp.where(i == 0, nx - (s - 2), s - 2), nx))
 
         lat_ring.step(s)
+        if s == min(2, far):
+            for k in reversed(order):
+                zm(k, True).wait_recv()
+            total = zmod[0]
+            for k in range(1, nz):
+                total = total + zmod[k]
+            xmod[t] = total
+            for k in range(1, nt):
+                xm(k, False).start()
     lat_ring.pair_step(far - 1)
 
     @pl.loop(0, 2 if far > 1 else 1)
@@ -291,6 +292,7 @@
         if k in (1, nx - 1):
             raw_last(0 if k == 1 else 1, False).start()
         raw_pair(k, False).start()
+    q_ring.step(1)
     for side in range(2):
         raw_last(side, True).wait_recv()
     raw_pair(opposite, False).start()
@@ -308,8 +310,9 @@
         packed = packed + pltpu.roll(loose[g * group:(g + 1) * group], g * crows, 1)
     kvp[z] = jnp.concatenate([packed, jnp.zeros((kvp.shape[1] - group, 128), F32)], axis=0).astype(BF)
     kr_half = ROTARY // 2
-    kv_chunks = [lambda p, c: kv.at[p, pl.ds(0, 2 * PLAIN)], lambda p, c: kvp.at[p],
-                 lambda p, c: kv.at[p, pl.ds(2 * PLAIN + kr_half, kr_half + VROWS)]]
+    top = 2 * PLAIN + kr_half
+    kv_chunks = [lambda p, c: kv.at[p, pl.ds(0, PLAIN)], lambda p, c: kv.at[p, pl.ds(PLAIN, PLAIN)], lambda p, c: kvp.at[p],
+                 lambda p, c: kv.at[p, pl.ds(top, kr_half + VALUE)], lambda p, c: kv.at[p, pl.ds(top + kr_half + VALUE, VALUE)]]
     kv_ring = Gather(nz, z, along_z, kv_chunks, kv_z)
     kv_ring.start()
 
@@ -367,13 +370,13 @@
     def pass_on(s, ch):
         for d in range(2):
             hop(d, s, ch, s).wait_recv()
-            if d == ch // 2:
+            if d == ch // 3:
                 hop(d, s, ch, s + 1).start()
             else:
                 @pl.when(s + 1 < reach)
                 def _():
                     hop(d, s, ch, s + 1).start()
-            if ch == 2:
+            if ch == 3:
                 kr_swap(d, s, False).start()
 
     def attend_block(n):
@@ -392,56 +395,71 @@
                 parts[g] = moved if parts[g] is None else parts[g] + moved
         kvc[:, tile * 128:(tile + 1) * 128] = jnp.concatenate(parts, axis=0).astype(BF)
 
-    slots = 2 * (reach - 1)
-    first = min(q_ring.reach, slots)
-
-    def done_after(i):
-        return jnp.clip(2 * (i - first + 1), 0, i)
+    slots = 4 * (reach - 1)
+    first = min(2, q_ring.reach - 1)
+    tiles = nz // 4
+
+    def done_after(j):
+        return jnp.clip(2 * (j - first + 1), 0, j)
+
+    def context_tiles():
+        for tile in range(tiles - 1):
+            unpack(tile)
+        attend(kvc[0:KROWS, 0:128 * (tiles - 1)], kvc[KROWS:KROWS + VROWS, 0:128 * (tiles - 1)], True)
 
     def kv_slot(i, carry):
-        s = i // 2 + 1
-
-        @pl.when(lax.rem(i, 2) == 0)
+        s = i // 4 + 1
+
+        @pl.when(lax.rem(i, 4) == 0)
         def _():
             pass_on(s, 0)
-            pass_on(s, 1)
 
             @pl.when(s > 1)
             def _():
                 for d in range(2):
                     kr_swap(d, s - 1, True).wait_recv()
 
-        @pl.when(lax.rem(i, 2) == 1)
+        @pl.when(lax.rem(i, 4) == 1)
         def _():
+            pass_on(s, 1)
             pass_on(s, 2)
 
-        for step in range(1, q_ring.reach + 1):
-            @pl.when(i == min(step, first) - 1)
+        for part_of in (2, 3):
+            @pl.when(lax.rem(i, 4) == part_of)
+            def _():
+                pass_on(s, part_of + 1)
+
+        for step in range(2, q_ring.reach + 1):
+            @pl.when(i == 2 * (step - 2))
             def _():
                 q_ring.step(step)
                 if step == q_ring.reach:
                     query_up()
 
-        @pl.loop(jnp.where(i >= first, done_after(i - 1), 0), jnp.where(i >= first, done_after(i), 0))
-        def _(n):
-            attend_block(n)
+        if tiles > 1:
+            @pl.when(i == slots - 4)
+            def _():
+                context_tiles()
+
+        @pl.when(lax.rem(i, 2) == 1)
+        def _():
+            j = i // 2
+
+            @pl.loop(jnp.where(j > first, done_after(j - 1), 0), jnp.where(j >= first, done_after(j), 0))
+            def _(n):
+                attend_block(n)
         return carry
 
     lax.fori_loop(0, slots, kv_slot, 0)
     for d in range(2):
         kr_swap(d, reach - 1, True).wait_recv()
 
-    @pl.loop(done_after(slots - 1), 2 * reach - 1)
+    @pl.loop(done_after(slots // 2 - 1), 2 * reach - 1)
     def _(n):
         attend_block(n)
-    tiles = nz // 4
-    for tile in range(tiles - 1):
-        unpack(tile)
-    if tiles > 1:
-        attend(kvc[0:KROWS, 0:128 * (tiles - 1)], kvc[KROWS:KROWS + VROWS, 0:128 * (tiles - 1)], True)
     kv_ring.ring_arrival(0, reach, 0).wait_recv()
-    kv_ring.ring_arrival(0, reach, 1).wait_recv()
-    kv_ring.ring_arrival(1, reach, 2).wait_recv()
+    for d, ch in ((0, 1), (0, 2), (1, 3), (1, 4)):
+        kv_ring.ring_arrival(d, reach, ch).wait_recv()
     kr_swap(0, reach, False).start()
     unpack(tiles - 1)
     kr_swap(0, reach, True).wait_recv()
@@ -528,7 +546,7 @@
         vm((tok, nt * VROWS), BF), vm((nt, rows, part), BF), vm((nt, rows, part), BF),
         vm((nt * rank_q, 1), F32), vm((nt * rank_kv, 1), F32), vm((4, 8, tok), F32),
         dma((9,)), dma((nz,)), dma((nz,)), dma((nt,)), dma((nt,)), dma((nt,)), dma((nt,)),
-        sems(nx, 4, True), dma((nx + 1,)), dma((nx + 1,)), dma((nx,)), dma((nx,)), sems(nx, 2, True), sems(nz, 3, False),
+        sems(nx, 4, True), dma((nx + 1,)), dma((nx + 1,)), dma((nx,)), dma((nx,)), sems(nx, 2, True), sems(nz, 5, False),
         dma((2, nz // 2 + 1)), dma((2, nz // 2 + 1)), sems(nx, 4, True),
     ]
     here = pl.BlockSpec(memory_space=vm)

time: 166 us -> 162 us (0.976)
  Pallas kernels: 164 us -> 160 us
    pallas_call x1, Pallas kernels: 164 us -> 160 us  [on_device(): pl.pallas_call(functools.partial(kernel, nz, nt), out_shape=(jax.ShapeDty...]
where the time goes in v5:
time: 162 us
  Pallas kernels  160 us (99%)
  other arithmetic  1.67 us (1%)
    pallas_call x1, Pallas kernels, on_device(): pl.pallas_call(functools.partial(kernel, nz, nt), out_shape=(jax.ShapeDty...  160 us

profile of v5, /device:TPU:65, one launch (start us, length us, event | category | flops | bytes accessed | tf_op | source)
XLA Modules:
  0.0 161.9 jit_solution(11767429360087712528)
XLA Ops:
  0.0 0.0 copy-start
  0.0 160.2 %block.1 = (bf16[24,4096]{1,0:T(8,128)(2,1)}, f32[1,4096]{1,0:T(1,128)}) custom-call(bf16[24,4096]{1,0:T(8,128)(2,1)} %refs_0_.1, f32[2,256]{1,0:T(2,128)} %refs_1_.1, bf16[32,4096]{1,0:T(8,128)(2,1)} %refs_2_.1, bf16[256,256]{1,0:T(8,128)(2,1)} %refs_3_.1, bf16[256,256]{1,0:T(8,128)(2,1)} %refs_4_.1, bf16[256,256]{1,0:T(8,128)(2,1)} %refs_5_.1, ...), custom_call_target="tpu_custom_call" | custom-call | tf_op jit(solution)/shard_map/block/pallas_call | solution.py:555
  160.2 0.0 copy-done
  160.3 1.7 %add_convert_fusion = bf16[24,4096]{1,0:T(8,128)(2,1)} fusion(bf16[24,4096]{1,0:T(8,128)(2,1)} %get-tuple-element.8, bf16[24,4096]{1,0:T(8,128)(2,1)S(1)} %copy-done, f32[4096]{0:T(1024)} %bitcast.12), kind=kLoop, calls=%fused_computation | loop fusion | flops 491520 | bytes 606208 | tf_op jit(solution)/shard_map/convert_element_type | solution.py:565
Async XLA Ops:
  0.0 160.2 %copy-start = (bf16[24,4096]{1,0:T(8,128)(2,1)S(1)}, bf16[24,4096]{1,0:T(8,128)(2,1)}, u32[]{:S(2)}) copy-start(bf16[24,4096]{1,0:T(8,128)(2,1)} %refs_0_.1) | copy-start | bytes 589828

commit v6 on v5

--- a/solution.py
+++ b/solution.py
@@ -469,9 +469,9 @@
     outT = jnp.concatenate([acc[0] / l_ref[0], acc[1] / l_ref[1]], axis=0)
     mine_at = lambda p, c: pl.ds(pl.multiple_of((2 * p + c) * VROWS, VROWS), VROWS)
     att[:, mine_at(chip, core)] = outT.T.astype(BF)
-    fourth = tok // 4
+    rows_of = tok // 8
     att_ring = Gather(nx, chip, along_x,
-                      [lambda p, c, i=i: att.at[pl.ds(i * fourth, fourth), mine_at(p, c)] for i in range(4)],
+                      [lambda p, c, i=i: att.at[pl.ds(i * rows_of, rows_of), mine_at(p, c)] for i in range(8)],
                       att_x, partner, core)
     att_ring.start()
     for s in range(1, att_ring.reach + 1):
@@ -547,7 +547,7 @@
         vm((nt * rank_q, 1), F32), vm((nt * rank_kv, 1), F32), vm((4, 8, tok), F32),
         dma((9,)), dma((nz,)), dma((nz,)), dma((nt,)), dma((nt,)), dma((nt,)), dma((nt,)),
         sems(nx, 4, True), dma((nx + 1,)), dma((nx + 1,)), dma((nx,)), dma((nx,)), sems(nx, 2, True), sems(nz, 5, False),
-        dma((2, nz // 2 + 1)), dma((2, nz // 2 + 1)), sems(nx, 4, True),
+        dma((2, nz // 2 + 1)), dma((2, nz // 2 + 1)), sems(nx, 8, True),
     ]
     here = pl.BlockSpec(memory_space=vm)
     away = pl.BlockSpec(memory_space=pl.ANY)

time: 162 us -> 164 us (1.012)
  Pallas kernels: 160 us -> 162 us
where the time goes in v6:
time: 164 us; the launch traced here: 163 us
  Pallas kernels  162 us (99%)
  other arithmetic  1.67 us (1%)
    pallas_call x1, Pallas kernels, on_device(): pl.pallas_call(functools.partial(kernel, nz, nt), out_shape=(jax.ShapeDty...  162 us

profile of v6, /device:TPU:65, one launch (start us, length us, event | category | flops | bytes accessed | tf_op | source)
XLA Modules:
  0.0 163.4 jit_solution(721696742997639212)
XLA Ops:
  0.0 0.0 copy-start
  0.0 161.7 %block.1 = (bf16[24,4096]{1,0:T(8,128)(2,1)}, f32[1,4096]{1,0:T(1,128)}) custom-call(bf16[24,4096]{1,0:T(8,128)(2,1)} %refs_0_.1, f32[2,256]{1,0:T(2,128)} %refs_1_.1, bf16[32,4096]{1,0:T(8,128)(2,1)} %refs_2_.1, bf16[256,256]{1,0:T(8,128)(2,1)} %refs_3_.1, bf16[256,256]{1,0:T(8,128)(2,1)} %refs_4_.1, bf16[256,256]{1,0:T(8,128)(2,1)} %refs_5_.1, ...), custom_call_target="tpu_custom_call" | custom-call | tf_op jit(solution)/shard_map/block/pallas_call | solution.py:555
  161.7 0.0 copy-done
  161.7 1.7 %add_convert_fusion = bf16[24,4096]{1,0:T(8,128)(2,1)} fusion(bf16[24,4096]{1,0:T(8,128)(2,1)} %get-tuple-element.8, bf16[24,4096]{1,0:T(8,128)(2,1)S(1)} %copy-done, f32[4096]{0:T(1024)} %bitcast.12), kind=kLoop, calls=%fused_computation | loop fusion | flops 491520 | bytes 606208 | tf_op jit(solution)/shard_map/convert_element_type | solution.py:565
Async XLA Ops:
  0.0 161.7 %copy-start = (bf16[24,4096]{1,0:T(8,128)(2,1)S(1)}, bf16[24,4096]{1,0:T(8,128)(2,1)}, u32[]{:S(2)}) copy-start(bf16[24,4096]{1,0:T(8,128)(2,1)} %refs_0_.1) | copy-start | bytes 589828

commit v7 on v5

--- a/solution.py
+++ b/solution.py
@@ -485,11 +485,18 @@
 
     for s in range(0, att_ring.reach + 1):
         att_ring.pair_step(s)
-    proj = jnp.dot(att[...], wo[...], preferred_element_type=F32)
-    for j in range(nt):
-        pbuf[j] = proj[j * rows:(j + 1) * rows].astype(BF)
-    for k in sorted(range(1, nt), key=lambda k: -min(k, nt - k)):
-        am(k, False).start()
+    peers = nt // 2
+    for part_of in range(2):
+        at = part_of * peers
+        proj = jnp.dot(att[at * rows:(at + peers) * rows, :], wo[...], preferred_element_type=F32)
+        for j in range(peers):
+            pbuf[at + j] = proj[j * rows:(j + 1) * rows].astype(BF)
+        for j in range(peers):
+            far_one = at + lax.rem(t + j, peers)
+
+            @pl.when(far_one != t)
+            def _():
+                am(lax.rem(far_one - t + nt, nt), False).start()
     mbuf[t] = pbuf[t]
     gate_ref[...] = mod[4:5, :]
     for k in range(1, nt):

time: 162 us -> 161 us (level)
  no operation moved by 1% of the time
where the time goes in v7:
time: 161 us
  Pallas kernels  159 us (99%)
  other arithmetic  1.67 us (1%)
    pallas_call x1, Pallas kernels, on_device(): pl.pallas_call(functools.partial(kernel, nz, nt), out_shape=(jax.ShapeDty...  159 us

profile of v7, /device:TPU:65, one launch (start us, length us, event | category | flops | bytes accessed | tf_op | source)
XLA Modules:
  0.0 160.8 jit_solution(2891930600421735461)
XLA Ops:
  0.0 0.0 copy-start
  0.0 159.1 %block.1 = (bf16[24,4096]{1,0:T(8,128)(2,1)}, f32[1,4096]{1,0:T(1,128)}) custom-call(bf16[24,4096]{1,0:T(8,128)(2,1)} %refs_0_.1, f32[2,256]{1,0:T(2,128)} %refs_1_.1, bf16[32,4096]{1,0:T(8,128)(2,1)} %refs_2_.1, bf16[256,256]{1,0:T(8,128)(2,1)} %refs_3_.1, bf16[256,256]{1,0:T(8,128)(2,1)} %refs_4_.1, bf16[256,256]{1,0:T(8,128)(2,1)} %refs_5_.1, ...), custom_call_target="tpu_custom_call" | custom-call | tf_op jit(solution)/shard_map/block/pallas_call | solution.py:562
  159.1 0.0 copy-done
  159.1 1.7 %add_convert_fusion = bf16[24,4096]{1,0:T(8,128)(2,1)} fusion(bf16[24,4096]{1,0:T(8,128)(2,1)} %get-tuple-element.8, bf16[24,4096]{1,0:T(8,128)(2,1)S(1)} %copy-done, f32[4096]{0:T(1024)} %bitcast.12), kind=kLoop, calls=%fused_computation | loop fusion | flops 491520 | bytes 606208 | tf_op jit(solution)/shard_map/convert_element_type | solution.py:572
Async XLA Ops:
  0.0 159.1 %copy-start = (bf16[24,4096]{1,0:T(8,128)(2,1)S(1)}, bf16[24,4096]{1,0:T(8,128)(2,1)}, u32[]{:S(2)}) copy-start(bf16[24,4096]{1,0:T(8,128)(2,1)} %refs_0_.1) | copy-start | bytes 589828
